TPU v7x, 32 devices: a whole 2x2x4 slice. The times are simulated.
32 devices in a mesh: sp: 8 (over z, y), tp: 4 (over x, core).
Axes of the slice: x: 2, y: 2, z: 4, core: 2. Of those that a mesh axis runs over, the one named last changes fastest.
Arguments:
- arriving_hidden_state: bfloat16 [8192, 2048], P(('sp', 'tp')), may hold values from -6 to 6
- former_request_vectors: bfloat16 [8192, 1024], P('sp', 'tp'), may hold values from -6 to 6
- former_match_vectors: bfloat16 [8192, 1024], P('sp', 'tp'), may hold values from -6 to 6
- latter_request_vectors: bfloat16 [8192, 512], P('sp', 'tp'), may hold values from -6 to 6
- latter_match_vectors: bfloat16 [8192, 512], P('sp', 'tp'), may hold values from -6 to 6
- stored_vectors_both: bfloat16 [8192, 2, 1024], P('sp', None, 'tp'), may hold values from -6 to 6
- closing_valve_operands: bfloat16 [8192, 2, 1024], P('sp', None, 'tp'), may hold values from -6 to 6
- update_level_before_squash: bfloat16 [2, 8, 8192], P(None, 'tp', 'sp'), may hold values from -4 to -3
- fading_data_input: float32 [2, 8, 8192], P(None, 'tp', 'sp'), may hold values from -5.5 to 5.5
- sparse_fading_boost: float32 [2, 8, 8192], P(None, 'tp', 'sp'), may hold values from -2 to 0, as said below
- unitwise_fading_loglevel: float32 [2, 8], P(None, 'tp'), as said below
- fading_constant_term: float32 [2, 8], P(None, 'tp'), may hold values from -1 to 1
- unitwise_normalizer_coef: float32 [128], replicated, may hold values from 0.1 to 1.9
- emission_map_weights: bfloat16 [2048, 2048], replicated, may hold values from -0.125 to 0.125
- channel_normalizer_coef: float32 [2048], replicated, may hold values from 0.1 to 1.9
- switching_channel_map: bfloat16 [2048, 6144], P('sp', 'tp'), may hold values from -0.125 to 0.125
- broadening_channel_map: bfloat16 [2048, 6144], P('sp', 'tp'), may hold values from -0.125 to 0.125
- timewise_convolve_tapvalues: bfloat16 [3, 2, 6144], P(None, None, 'tp'), may hold values from -3.5 to 3.5
- narrowing_map_weights_in: bfloat16 [2048, 6144], P('sp', 'tp'), may hold values from -0.078125 to 0.078125
Outputs:
- mixed: bfloat16 [8192, 2048], P(('sp', 'tp'))
Inputs may be any that keep to these rules, and one draw needn't show every extreme that they name: `unitwise_fading_loglevel`: each entry is the logarithm of a per-position rate between 0.2 / 8192 and 2 / 64. `sparse_fading_boost`: zero except at three or fewer positions of the sequence.
All inputs are finite; a program needn't handle non-finite values.
Results may differ from a plain program's by a relative error of at most 0.015.
Values may be sent and summed in bfloat16 or wider, within the bound.
A program may use at most 128 MiB of HBM per device.

v0:
```python
import functools

import jax
import jax.numpy as jnp
from jax import lax
from jax.experimental import pallas as pl
from jax.experimental.pallas import tpu as pltpu
from jax.sharding import PartitionSpec as P


TAPS = 3
CHUNK = 128
BASE = 16
LANES = 128

EPSILON = 1e-06
F32 = jnp.float32
BF16 = jnp.bfloat16


def from_behind(value, axis, steps):
    count = lax.axis_size(axis)
    leading, last = (max(0, -steps), min(count, count - steps))
    return lax.ppermute(value, axis, [(source, source + steps) for source in range(leading, last)])


def mm(a, b):
    return jnp.dot(a.astype(BF16), b.astype(BF16), preferred_element_type=F32)


def mm_nt(a, b):
    return lax.dot_general(
        a.astype(BF16), b.astype(BF16), (((1,), (1,)), ((), ())), preferred_element_type=F32
    )


def mm_tn(a, b):
    return mm(a.T, b)


def local_kernel(
    q1_ref, k1_ref, q2_ref, k2_ref, v_ref, gb_ref, from_ref, *rest
):
    g_ref, h_ref, last_ref, sum_ref, run_ref = rest[-5:]
    step = pl.program_id(0)
    count = v_ref.shape[1] // LANES // 2
    pair = 2
    rows = lax.broadcasted_iota(jnp.int32, (CHUNK, CHUNK), 0)
    cols = lax.broadcasted_iota(jnp.int32, (CHUNK, CHUNK), 1)
    eye = (rows == cols).astype(F32)
    causal = rows >= cols
    strict = rows > cols
    lane = lax.broadcasted_iota(jnp.int32, (1, LANES), 1)

    @pl.when(step == 0)
    def _():
        run_ref[...] = from_ref[...]

    gb = gb_ref[...]
    cum = gb
    lanes8 = lax.broadcasted_iota(jnp.int32, gb.shape, 1)
    shift = 1
    while shift < CHUNK:
        cum = cum + jnp.where(lanes8 >= shift, pltpu.roll(cum, shift, 1), 0.0)
        shift *= 2
    gbt = gb.T
    cumt = cum.T

    pend = None
    for head in range(2 * count):
        group, at = head // count, head % count
        if group == 0:
            q = q1_ref[:, at * LANES : (at + 1) * LANES].astype(F32)
            k = k1_ref[:, at * LANES : (at + 1) * LANES].astype(F32)
            key_size = LANES
            own = None
        else:
            key_size = LANES // 2
            own = (lane // key_size) == at % pair
            first = (at // pair) * LANES
            q = jnp.where(own, q2_ref[:, first : first + LANES].astype(F32), 0.0)
            k = jnp.where(own, k2_ref[:, first : first + LANES].astype(F32), 0.0)
        q = q * (lax.rsqrt(jnp.sum(q * q, axis=-1, keepdims=True) + EPSILON) * key_size ** (-0.5))
        k = k * lax.rsqrt(jnp.sum(k * k, axis=-1, keepdims=True) + EPSILON)
        v = v_ref[:, head * LANES : (head + 1) * LANES].astype(F32)
        beta = gbt[:, 2 * count + head : 2 * count + head + 1]
        cum_col = cumt[:, head : head + 1]
        cum_row = cum[head : head + 1, :]
        total = cum[head : head + 1, CHUNK - 1 : CHUNK]
        decay = jnp.exp(jnp.where(causal, cum_col - cum_row, -1e30))
        grown = jnp.exp(cum_col)
        kbeta = k * beta
        kbf = k.astype(BF16)
        low = jnp.where(strict, mm_nt(kbeta, kbf) * decay, 0.0)
        intra = mm_nt(q, kbf) * decay
        base = jnp.where((rows // BASE) == (cols // BASE), low, 0.0)
        power = -base
        inv = eye + power
        size = 2
        while size < BASE:
            power = mm(power, power)
            inv = inv + mm(inv, power)
            size *= 2
        block = BASE
        while block < CHUNK:
            off = jnp.where(
                ((rows // (2 * block)) == (cols // (2 * block)))
                & ((rows // block) != (cols // block)),
                low,
                0.0,
            )
            inv = inv - mm(mm(inv, off), inv)
            block *= 2
        right = jnp.concatenate([v * beta, kbeta * grown], axis=-1)
        solved = mm(inv, right)
        kdec = k * jnp.exp(total - cum_col)
        both = mm_tn(kdec, solved)
        inner = mm(intra, solved)
        unit_diag = eye if own is None else jnp.where(own, eye, 0.0)
        cmap = jnp.exp(total) * unit_diag - both[:, LANES:]
        cadd = both[:, :LANES]
        pmat = q * grown - inner[:, LANES:]
        unit = head if group == 0 else count + at // pair
        run = run_ref[unit]
        seen = mm(pmat, run)
        h_ref[:, head * LANES : (head + 1) * LANES] = seen[:, :LANES] + inner[:, :LANES]
        g_ref[:, head * LANES : (head + 1) * LANES] = seen[:, LANES:].astype(g_ref.dtype)
        if pend is not None:
            cmap = cmap + pend[0]
            cadd = cadd + pend[1]
            pend = None
        if group == 1 and at % pair != pair - 1 and at != count - 1:
            pend = (cmap, cadd)
            continue
        nxt = mm(cmap, run)
        run_ref[unit, :, :LANES] = nxt[:, :LANES] + cadd
        run_ref[unit, :, LANES:] = nxt[:, LANES:]

    @pl.when(step == pl.num_programs(0) - 1)
    def _():
        last_ref[...] = run_ref[...]
        sum_ref[...] = run_ref[...].astype(sum_ref.dtype)


def local_terms(q1, k1, q2, k2, values, gates_beta, running, part, parts, earlier):
    length = q1.shape[0]
    wide = values.shape[1]
    steps = length // CHUNK // parts
    base = part * steps
    units = running.shape[0]
    whole = pl.BlockSpec((units, LANES, 2 * LANES), lambda i: (0, 0, 0))
    return pl.pallas_call(
        local_kernel,
        grid=(steps,),
        in_specs=[
            pl.BlockSpec((CHUNK, q1.shape[1]), lambda i: (i + base, 0)),
            pl.BlockSpec((CHUNK, k1.shape[1]), lambda i: (i + base, 0)),
            pl.BlockSpec((CHUNK, q2.shape[1]), lambda i: (i + base, 0)),
            pl.BlockSpec((CHUNK, k2.shape[1]), lambda i: (i + base, 0)),
            pl.BlockSpec((CHUNK, wide), lambda i: (i + base, 0)),
            pl.BlockSpec((gates_beta.shape[0], CHUNK), lambda i: (0, i + base)),
            whole,
        ]
        + [pl.BlockSpec(memory_space=pl.ANY)] * len(earlier),
        out_specs=[
            pl.BlockSpec((CHUNK, wide), lambda i: (i + base, 0)),
            pl.BlockSpec((CHUNK, wide), lambda i: (i + base, 0)),
            whole,
            whole,
        ],
        out_shape=[
            jax.ShapeDtypeStruct((length, wide), BF16),
            jax.ShapeDtypeStruct((length, wide), F32),
            jax.ShapeDtypeStruct((units, LANES, 2 * LANES), F32),
            jax.ShapeDtypeStruct((units, LANES, 2 * LANES), BF16),
        ],
        scratch_shapes=[pltpu.VMEM((units, LANES, 2 * LANES), F32)],
        input_output_aliases={7 + i: i for i in range(len(earlier))},
        cost_estimate=pl.CostEstimate(
            flops=steps * 4 * 400 * CHUNK**3, bytes_accessed=length * wide * 10, transcendentals=0
        ),
    )(q1, k1, q2, k2, values, gates_beta, running, *earlier)


def exchange_kernel(own_ref, all_ref, send_sem, recv_sem):
    me = lax.axis_index("sp")
    count = all_ref.shape[0]
    barrier = pltpu.get_barrier_semaphore()
    for gap in range(1, count):
        pl.semaphore_signal(
            barrier,
            inc=1,
            device_id={"sp": lax.rem(me + gap, count)},
            device_id_type=pl.DeviceIdType.MESH,
        )
    pl.semaphore_wait(barrier, count - 1)

    def copy(source, target):
        return pltpu.make_async_remote_copy(
            src_ref=own_ref,
            dst_ref=all_ref.at[source],
            send_sem=send_sem.at[target],
            recv_sem=recv_sem.at[source],
            device_id={"sp": target},
            device_id_type=pl.DeviceIdType.MESH,
        )

    for target in range(1, count):
        @pl.when(me < target)
        def _():
            copy(me, target).start()

    for source in range(count - 1):
        @pl.when(source < me)
        def _():
            copy(source, me).wait_recv()

    for target in range(1, count):
        @pl.when(me < target)
        def _():
            copy(me, target).wait_send()


def exchange(summary):
    count = lax.axis_size("sp")
    return pl.pallas_call(
        exchange_kernel,
        in_specs=[pl.BlockSpec(memory_space=pltpu.VMEM)],
        out_specs=pl.BlockSpec(memory_space=pltpu.VMEM),
        out_shape=jax.ShapeDtypeStruct((count, *summary.shape), summary.dtype),
        scratch_shapes=[pltpu.SemaphoreType.DMA((count,)), pltpu.SemaphoreType.DMA((count,))],
        compiler_params=pltpu.CompilerParams(collective_id=1, has_side_effects=True),
        cost_estimate=pl.CostEstimate(flops=10**9, bytes_accessed=10**6, transcendentals=0),
    )(summary)


def swapped(value, low, high):
    places = [2 * place + parity for place in range(low, high) for parity in range(2)]
    return lax.ppermute(value, "sp", [(i, i ^ 1) for i in places])


def line_start(own):
    ring = lax.axis_size("sp") // 2
    return dict(
        right=own, left=own, pieces=[(0, 0, 0, ring, own), (0, 1, 0, ring, swapped(own, 0, ring))]
    )


def line_step(line, gap):
    ring = lax.axis_size("sp") // 2
    if gap >= ring:
        return line
    up = [(2 * p + q, 2 * p + 2 + q) for p in range(gap - 1, ring - 1) for q in range(2)]
    down = [(2 * p + q, 2 * p - 2 + q) for p in range(1, ring - gap + 1) for q in range(2)]
    right = lax.ppermute(line["right"], "sp", up)
    left = lax.ppermute(line["left"], "sp", down)
    pieces = [(gap, 0, gap, ring, right), (ring - gap, 0, 0, ring - gap, left)]
    return dict(right=right, left=left, pieces=line["pieces"] + pieces)


def line_swap(line, gap):
    ring = lax.axis_size("sp") // 2
    if gap >= ring:
        return line
    pieces = [
        (gap, 1, gap, ring, swapped(line["right"], gap, ring)),
        (ring - gap, 1, 0, ring - gap, swapped(line["left"], 0, ring - gap)),
    ]
    return dict(line, pieces=line["pieces"] + pieces)


def line_rest(line, gap):
    ring = lax.axis_size("sp") // 2
    for more in range(gap, ring):
        line = line_swap(line_step(line, more), more)
    return line


def tie(line, other):
    other, right, left = lax.optimization_barrier((other, line["right"], line["left"]))
    return dict(line, right=right, left=left), other


def load_pieces(meta, refs, ranges, targets, sem):
    me = lax.axis_index("sp")
    ring = lax.axis_size("sp") // 2
    place = me // 2
    copies = []
    for (gap, other, low_place, high_place), ref in zip(meta, refs):
        owner = lax.rem(place + ring - gap, ring) * 2 + (lax.rem(me, 2) + other) % 2
        valid = (place >= low_place) & (place < high_place)
        for index, (low, high) in enumerate(ranges):
            size = high - low
            one = pltpu.make_async_copy(
                ref.at[pl.ds(low, size), :],
                targets[index].at[pl.ds(pl.multiple_of(owner * size, 16), size), :],
                sem.at[len(copies)],
            )
            copies.append((valid, one))

    for valid, one in copies:
        @pl.when(valid)
        def _():
            one.start()

    return copies


def finish_pieces(copies):
    for valid, one in copies:
        @pl.when(valid)
        def _():
            one.wait()


def project_kernel(x_ref, w_ref, skip_ref, coef_ref, sum_ref, out_ref):
    step = pl.program_id(0)

    @pl.when(step == 0)
    def _():
        sum_ref[...] = skip_ref[...].astype(F32)

    sum_ref[...] += jnp.dot(x_ref[...], w_ref[...], preferred_element_type=F32)

    @pl.when(step == pl.num_programs(0) - 1)
    def _():
        total = sum_ref[...]
        scale = lax.rsqrt(jnp.mean(total * total, axis=-1, keepdims=True) + EPSILON)
        out_ref[...] = (total * scale * coef_ref[...]).astype(out_ref.dtype)


def project(x, weights, skip, coef):
    rows, depth = x.shape
    width = weights.shape[1]
    part = min(512, depth)
    whole = pl.BlockSpec((rows, width), lambda i: (0, 0))
    return pl.pallas_call(
        project_kernel,
        grid=(depth // part,),
        in_specs=[
            pl.BlockSpec((rows, part), lambda i: (0, i)),
            pl.BlockSpec((part, width), lambda i: (i, 0)),
            whole,
            pl.BlockSpec((1, width), lambda i: (0, 0)),
        ],
        out_specs=[whole, whole],
        out_shape=[
            jax.ShapeDtypeStruct((rows, width), F32),
            jax.ShapeDtypeStruct((rows, width), BF16),
        ],
        cost_estimate=pl.CostEstimate(
            flops=2 * rows * depth * width, bytes_accessed=2 * depth * width, transcendentals=0
        ),
    )(x, weights, skip, coef)


def up_kernel(meta, x_ref, halo_ref, taps_ref, *rest):
    *refs, out_ref, gate_w, up_w, xs, sem = rest
    tile = x_ref.shape[0]
    step = pl.program_id(0)
    edge = halo_ref.shape[0]
    rows = gate_w.shape[0] // lax.axis_size("sp")

    @pl.when(step == 0)
    def _():
        copies = load_pieces(meta, refs, ((0, rows), (rows, 2 * rows)), (gate_w, up_w), sem)
        xs[:edge, :] = halo_ref[...]
        finish_pieces(copies)

    @pl.when(step > 0)
    def _():
        xs[:edge, :] = xs[tile:, :]

    xs[edge:, :] = x_ref[...]
    wide = out_ref.shape[1]
    part = min(256, wide)
    for col in range(0, wide, part):
        at = slice(col, col + part)
        taken = []
        for which, w in enumerate((gate_w, up_w)):
            low = jnp.dot(xs[...], w[:, at], preferred_element_type=F32)
            low = low.astype(BF16).astype(F32)
            total = 0.0
            for tap in range(TAPS):
                moved = low[edge - TAPS + 1 + tap : edge - TAPS + 1 + tap + tile]
                total = total + taps_ref[2 * tap + which : 2 * tap + which + 1, at] * moved
            taken.append(total)
        gate, up = taken
        out_ref[:, at] = (gate / (1.0 + jnp.exp(-gate)) * up).astype(out_ref.dtype)


def up_part(features, halo, taps, pieces):
    length, width = features.shape
    wide = taps.shape[1]
    tile = min(512, length)
    meta = [p[:4] for p in pieces]
    arrays = [p[4] for p in pieces]
    edge = halo.shape[0]
    return pl.pallas_call(
        functools.partial(up_kernel, meta),
        grid=(length // tile,),
        in_specs=[
            pl.BlockSpec((tile, width), lambda i: (i, 0)),
            pl.BlockSpec(halo.shape, lambda i: (0, 0)),
            pl.BlockSpec(taps.shape, lambda i: (0, 0)),
        ]
        + [pl.BlockSpec(memory_space=pl.ANY)] * len(arrays),
        out_specs=pl.BlockSpec((tile, wide), lambda i: (i, 0)),
        out_shape=jax.ShapeDtypeStruct((length, wide), BF16),
        scratch_shapes=[
            pltpu.VMEM((width, wide), BF16),
            pltpu.VMEM((width, wide), BF16),
            pltpu.VMEM((tile + edge, width), BF16),
            pltpu.SemaphoreType.DMA((2 * len(arrays),)),
        ],
        compiler_params=pltpu.CompilerParams(vmem_limit_bytes=50 * 2**20),
        cost_estimate=pl.CostEstimate(
            flops=4 * length * width * wide, bytes_accessed=4 * width * wide, transcendentals=0
        ),
    )(features, halo, taps, *arrays)


def down_kernel(meta, x_ref, *rest):
    *refs, out_ref, down_w, sem = rest
    rows = down_w.shape[0] // lax.axis_size("sp")

    @pl.when(pl.program_id(0) == 0)
    def _():
        copies = load_pieces(meta, refs, ((0, rows),), (down_w,), sem)
        finish_pieces(copies)

    wide = out_ref.shape[1]
    part = min(512, wide)
    for col in range(0, wide, part):
        out_ref[:, col : col + part] = mm_nt(x_ref[...], down_w[col : col + part, :]).astype(BF16)


def down_part(hidden, width, pieces):
    length, wide = hidden.shape
    tile = min(512, length)
    meta = [p[:4] for p in pieces]
    arrays = [p[4] for p in pieces]
    return pl.pallas_call(
        functools.partial(down_kernel, meta),
        grid=(length // tile,),
        in_specs=[pl.BlockSpec((tile, wide), lambda i: (i, 0))]
        + [pl.BlockSpec(memory_space=pl.ANY)] * len(arrays),
        out_specs=pl.BlockSpec((tile, width), lambda i: (i, 0)),
        out_shape=jax.ShapeDtypeStruct((length, width), BF16),
        scratch_shapes=[
            pltpu.VMEM((width, wide), BF16),
            pltpu.SemaphoreType.DMA((len(arrays),)),
        ],
        compiler_params=pltpu.CompilerParams(vmem_limit_bytes=50 * 2**20),
        cost_estimate=pl.CostEstimate(
            flops=2 * length * width * wide, bytes_accessed=2 * width * wide, transcendentals=0
        ),
    )(hidden, *arrays)


def finish_kernel(place_ref, all_ref, g_ref, h_ref, gate_ref, coef_ref, out_ref, state_ref):
    @pl.when(pl.program_id(0) == 0)
    def _():
        state_ref[...] = jnp.zeros_like(state_ref)

        def turn(i, carry):
            for unit in range(all_ref.shape[1]):
                block = all_ref[i, unit]
                state_ref[unit] = (
                    mm(block[:, LANES:], state_ref[unit]) + block[:, :LANES].astype(F32)
                )
            return carry

        lax.fori_loop(0, place_ref[0], turn, 0)

    coef = coef_ref[...]
    count = out_ref.shape[1] // LANES // 2
    for head in range(2 * count):
        unit = head if head < count else count + (head - count) // 2
        at = pl.ds(head * LANES, LANES)
        out = mm(g_ref[:, at], state_ref[unit]) + h_ref[:, at]
        gate = gate_ref[:, at].astype(F32)
        scaled = out * lax.rsqrt(jnp.mean(out * out, axis=-1, keepdims=True) + EPSILON) * coef
        out_ref[:, at] = (scaled * (gate / (1.0 + jnp.exp(-gate)))).astype(out_ref.dtype)


def finish_heads(place, everyone, g, h, gates, coef):
    length, wide = g.shape
    tile = min(256, length)
    return pl.pallas_call(
        finish_kernel,
        grid_spec=pltpu.PrefetchScalarGridSpec(
            num_scalar_prefetch=1,
            grid=(length // tile,),
            in_specs=[
                pl.BlockSpec(everyone.shape, lambda i, p: (0, 0, 0, 0)),
                pl.BlockSpec((tile, wide), lambda i, p: (i, 0)),
                pl.BlockSpec((tile, wide), lambda i, p: (i, 0)),
                pl.BlockSpec((tile, wide), lambda i, p: (i, 0)),
                pl.BlockSpec((1, LANES), lambda i, p: (0, 0)),
            ],
            out_specs=pl.BlockSpec((tile, wide), lambda i, p: (i, 0)),
            scratch_shapes=[pltpu.VMEM((everyone.shape[1], LANES, LANES), F32)],
        ),
        out_shape=jax.ShapeDtypeStruct((length, wide), BF16),
        cost_estimate=pl.CostEstimate(
            flops=2 * length * wide * LANES * 8, bytes_accessed=length * wide * 10, transcendentals=0
        ),
    )(place, everyone, g, h, gates, coef)


def per_device(
    arriving_hidden_state,
    former_request_vectors,
    former_match_vectors,
    latter_request_vectors,
    latter_match_vectors,
    stored_vectors_both,
    closing_valve_operands,
    update_level_before_squash,
    fading_data_input,
    sparse_fading_boost,
    unitwise_fading_loglevel,
    fading_constant_term,
    unitwise_normalizer_coef,
    emission_map_weights,
    channel_normalizer_coef,
    switching_channel_map,
    broadening_channel_map,
    timewise_convolve_tapvalues,
    narrowing_map_weights_in,
):
    length = former_request_vectors.shape[0]
    level = (
        -jnp.exp(unitwise_fading_loglevel)[..., None]
        * jax.nn.softplus(fading_data_input + fading_constant_term[..., None])
        + sparse_fading_boost
    )
    beta_rate = jax.nn.sigmoid(update_level_before_squash.astype(jnp.float32))
    gates_beta = jnp.concatenate([level, beta_rate], axis=0).reshape(-1, length)
    gates_beta = jnp.pad(gates_beta, ((0, -gates_beta.shape[0] % 8), (0, 0)))
    spare = -latter_request_vectors.shape[1] % LANES
    sides = jnp.concatenate([switching_channel_map, broadening_channel_map], axis=0)
    side = line_step(line_start(sides), 1)
    units = former_request_vectors.shape[1] // LANES + (
        latter_request_vectors.shape[1] + spare
    ) // LANES
    running = jnp.broadcast_to(jnp.eye(LANES, 2 * LANES, LANES, dtype=F32), (units, LANES, 2 * LANES))
    drawn = (
        former_request_vectors,
        former_match_vectors,
        jnp.pad(latter_request_vectors, ((0, 0), (0, spare))),
        jnp.pad(latter_match_vectors, ((0, 0), (0, spare))),
        stored_vectors_both.reshape(length, -1),
        gates_beta,
    )
    parts = 4 if length % (4 * CHUNK) == 0 else 1
    done = ()
    summary = None
    for part in range(parts):
        if part == parts // 2:
            side, running = tie(side, running)
            side = line_step(line_swap(side, 1), 2)
        *done, running, summary = local_terms(*drawn, running, part, parts, tuple(done))
    g_part, h_part = done
    everyone = exchange(summary)
    side, (everyone, narrow) = tie(side, (everyone, narrowing_map_weights_in))
    side = line_step(line_swap(side, 2), 3)
    down = line_step(line_start(narrow), 1)
    place = lax.axis_index("sp").astype(jnp.int32).reshape(1)
    attended = finish_heads(
        place,
        everyone,
        g_part,
        h_part,
        closing_valve_operands.reshape(length, -1),
        unitwise_normalizer_coef.reshape(1, -1),
    )
    linear_attend = attended.reshape(length, 2, -1)
    arrived = lax.all_to_all(linear_attend, "tp", split_axis=0, concat_axis=2, tiled=True)
    row_count = arrived.shape[0]
    skip_stream, normed = project(
        arrived.reshape(row_count, -1),
        emission_map_weights,
        arriving_hidden_state,
        channel_normalizer_coef.reshape(1, -1),
    )
    side, normed = tie(side, normed)
    side = line_rest(line_swap(side, 3), 4)
    features = lax.all_gather(normed, "tp", axis=0, tiled=True)
    down = line_step(line_swap(down, 1), 2)
    edge = 16
    halo = from_behind(features[-edge:], "sp", 1)
    taps = timewise_convolve_tapvalues.astype(F32).reshape(2 * TAPS, -1)
    down, halo = tie(down, halo)
    down = line_step(line_swap(down, 2), 3)
    hidden = up_part(features, halo, taps, side["pieces"])
    down = line_rest(line_swap(down, 3), 4)
    down_sum = lax.psum_scatter(
        down_part(hidden, features.shape[1], down["pieces"]),
        "tp",
        scatter_dimension=0,
        tiled=True,
    ).astype(jnp.float32)
    return (skip_stream + down_sum).astype(jnp.bfloat16)


def solution(mesh):
    placed = (
        P(("sp", "tp"), None),
        P("sp", "tp"),
        P("sp", "tp"),
        P("sp", "tp"),
        P("sp", "tp"),
        P("sp", None, "tp"),
        P("sp", None, "tp"),
        P(None, "tp", "sp"),
        P(None, "tp", "sp"),
        P(None, "tp", "sp"),
        P(None, "tp"),
        P(None, "tp"),
        P(),
        P(),
        P(),
        P("sp", "tp"),
        P("sp", "tp"),
        P(None, None, "tp"),
        P("sp", "tp"),
    )
    return jax.shard_map(
        per_device, mesh=mesh, in_specs=placed, out_specs=P(("sp", "tp"), None), check_vma=False
    )
```

profile of v0, /device:TPU:0, one launch (start us, length us, event | category | flops | bytes accessed | tf_op | source)
XLA Modules:
  0.0 458.1 jit_solution(11120098657306355490)
XLA Ops:
  6.5 1.3 constant_dynamic-update-slice_fusion.1
  8.0 6.1 %collective-permute-start = (bf16[512,1536]{1,0:T(8,128)(2,1)S(1)}, bf16[512,1536]{1,0:T(8,128)(2,1)}, u32[]{:S(2)}, u32[]{:S(2)}) collective-permute-start(bf16[512,1536]{1,0:T(8,128)(2,1)S(1)} %constant_dynamic-update-slice_fusion.rest_0_), channel_id=1, source_target_pairs={{0,8},{4,12},{8,16},{12,20},{16,24},{20,28},{1,9},{5,13},{9,17},{1... | collective-permute-start | bytes 4718600 | tf_op jit(solution)/shard_map/ppermute | solution.py:255
  14.1 1.3 collective-permute-start.1
  15.4 1.2 copy.30
  18.3 17.4 %shard_map.181 = (bf16[1024,512]{1,0:T(8,128)(2,1)}, f32[1024,512]{1,0:T(8,128)}, f32[3,128,256]{2,1,0:T(8,128)}, bf16[3,128,256]{2,1,0:T(8,128)(2,1)}) custom-call(bf16[1024,256]{1,0:T(8,128)(2,1)} %q1_ref.7, bf16[1024,256]{1,0:T(8,128)(2,1)} %k1_ref.7, bf16[1024,128]{1,0:T(8,128)(2,1)} %q2_ref.7, bf16[1024,128]{1,0:T(8,128)(2,1)} %k2_ref.7, ...), custom_call_target="tpu_custom_call" | custom-call | flops 6710886400 | bytes 5242880 | tf_op jit(solution)/shard_map/pallas_call | solution.py:152
  35.7 17.3 %shard_map.182 = (bf16[1024,512]{1,0:T(8,128)(2,1)}, f32[1024,512]{1,0:T(8,128)}, f32[3,128,256]{2,1,0:T(8,128)}, bf16[3,128,256]{2,1,0:T(8,128)(2,1)}) custom-call(bf16[1024,256]{1,0:T(8,128)(2,1)} %q1_ref.7, bf16[1024,256]{1,0:T(8,128)(2,1)} %k1_ref.7, bf16[1024,128]{1,0:T(8,128)(2,1)} %q2_ref.7, ...), custom_call_target="tpu_custom_call", output_to_operand_aliasing={{0}: (7, {}), {1}: (8, {})} | custom-call | flops 6710886400 | bytes 5242880 | tf_op jit(solution)/shard_map/pallas_call | solution.py:152
  53.0 1.8 collective-permute-start.2
  54.8 1.3 collective-permute-start.3
  56.1 17.4 %shard_map.183 = (bf16[1024,512]{1,0:T(8,128)(2,1)}, f32[1024,512]{1,0:T(8,128)}, f32[3,128,256]{2,1,0:T(8,128)}, bf16[3,128,256]{2,1,0:T(8,128)(2,1)}) custom-call(bf16[1024,256]{1,0:T(8,128)(2,1)} %q1_ref.7, bf16[1024,256]{1,0:T(8,128)(2,1)} %k1_ref.7, bf16[1024,128]{1,0:T(8,128)(2,1)} %q2_ref.7, ...), custom_call_target="tpu_custom_call", output_to_operand_aliasing={{0}: (7, {}), {1}: (8, {})} | custom-call | flops 6710886400 | bytes 5242880 | tf_op jit(solution)/shard_map/pallas_call | solution.py:152
  73.5 17.4 %shard_map.184 = (bf16[1024,512]{1,0:T(8,128)(2,1)}, f32[1024,512]{1,0:T(8,128)}, f32[3,128,256]{2,1,0:T(8,128)}, bf16[3,128,256]{2,1,0:T(8,128)(2,1)}) custom-call(bf16[1024,256]{1,0:T(8,128)(2,1)} %q1_ref.7, bf16[1024,256]{1,0:T(8,128)(2,1)} %k1_ref.7, bf16[1024,128]{1,0:T(8,128)(2,1)} %q2_ref.7, ...), custom_call_target="tpu_custom_call", output_to_operand_aliasing={{0}: (7, {}), {1}: (8, {})} | custom-call | flops 6710886400 | bytes 5242880 | tf_op jit(solution)/shard_map/pallas_call | solution.py:152
  90.9 35.0 %shard_map.185.all_ref = bf16[8,3,128,256]{3,2,1,0:T(8,128)(2,1)} custom-call(bf16[3,128,256]{2,1,0:T(8,128)(2,1)} %get-tuple-element.42.own_ref), custom_call_target="tpu_custom_call" | custom-call | flops 1000000000 | bytes 1000000 | tf_op jit(solution)/shard_map/pallas_call | solution.py:226
  125.9 1.8 collective-permute-start.4
  127.7 1.5 collective-permute-start.5
  129.2 1.2 copy.31
  130.4 5.5 %shard_map.186 = bf16[1024,512]{1,0:T(8,128)(2,1)} custom-call(s32[1]{0:T(128)} %bitcast.place_ref, bf16[8,3,128,256]{3,2,1,0:T(8,128)(2,1)} %shard_map.185.all_ref, bf16[1024,512]{1,0:T(8,128)(2,1)} %get-tuple-element.46.g_ref, f32[1024,512]{1,0:T(8,128)} %get-tuple-element.47.h_ref, bf16[1024,512]{1,0:T(8,128)(2,1)} %bitcast.11, f32[1,128]{1,0:T(1,128)} %bitcast.19), custom_call_target="tpu_custom_call" | custom-call | flops 1073741824 | bytes 5242880 | tf_op jit(solution)/shard_map/pallas_call | solution.py:490
  135.9 1.3 reshape.38
  137.2 17.0 %all_to_all.15 = bf16[1024,2,256]{2,1,0:T(2,128)(2,1)S(1)} all-to-all(bf16[1024,2,256]{2,1,0:T(2,128)(2,1)S(1)} %reshape.38), channel_id=1, replica_groups=mesh['sp'=8,'tp'=4] {'tp'}, dimensions={0} | all-to-all | bytes 2097152 | tf_op jit(solution)/shard_map/all_to_all | solution.py:580
  155.2 1.6 reshape.39.x_ref
  156.8 8.2 %shard_map.187 = (f32[256,2048]{1,0:T(8,128)}, bf16[256,2048]{1,0:T(8,128)(2,1)}) custom-call(bf16[256,2048]{1,0:T(8,128)(2,1)} %reshape.39.x_ref, bf16[2048,2048]{1,0:T(8,128)(2,1)} %w_ref.1, bf16[256,2048]{1,0:T(8,128)(2,1)} %skip_ref.1, f32[1,2048]{1,0:T(1,128)} %bitcast.18), custom_call_target="tpu_custom_call" | custom-call | flops 2147483648 | bytes 8388608 | tf_op jit(solution)/shard_map/pallas_call | solution.py:337
  165.0 5.7 %collective-permute-done.5.rest_11_ = bf16[512,1536]{1,0:T(8,128)(2,1)} collective-permute-done((bf16[512,1536]{1,0:T(8,128)(2,1)}, bf16[512,1536]{1,0:T(8,128)(2,1)}, u32[]{:S(2)}, u32[]{:S(2)}) %collective-permute-start.5) | collective-permute-done | bytes 1572896 | tf_op jit(solution)/shard_map/ppermute | solution.py:256
  172.1 3.4 collective-permute-start.13
  175.5 8.4 %collective-permute-start.7 = (bf16[256,1536]{1,0:T(8,128)(2,1)}, bf16[256,1536]{1,0:T(8,128)(2,1)S(1)}, u32[]{:S(2)}, u32[]{:S(2)}) collective-permute-start(bf16[256,1536]{1,0:T(8,128)(2,1)} %rest_0_), channel_id=1, source_target_pairs={{0,8},{4,12},{8,16},{12,20},{16,24},{20,28},{1,9},{5,13},{9,17},{1... | collective-permute-start | bytes 2359304 | tf_op jit(solution)/shard_map/ppermute | solution.py:255
  183.9 1.3 collective-permute-start.9
  185.2 22.9 %collective-permute-done.11.rest_1_ = bf16[512,1536]{1,0:T(8,128)(2,1)S(1)} collective-permute-done((bf16[512,1536]{1,0:T(8,128)(2,1)S(1)}, bf16[512,1536]{1,0:T(8,128)(2,1)S(1)}, u32[]{:S(2)}, u32[]{:S(2)}) %collective-permute-start.11) | collective-permute-done | bytes 1572896 | tf_op jit(solution)/shard_map/ppermute | solution.py:239
  208.6 0.9 copy-done.1
  210.3 1.8 collective-permute-start.14
  212.1 29.7 %collective-permute-done.13.rest_5_ = bf16[512,1536]{1,0:T(8,128)(2,1)S(1)} collective-permute-done((bf16[512,1536]{1,0:T(8,128)(2,1)}, bf16[512,1536]{1,0:T(8,128)(2,1)S(1)}, u32[]{:S(2)}, u32[]{:S(2)}) %collective-permute-start.13) | collective-permute-done | bytes 1572896 | tf_op jit(solution)/shard_map/ppermute | solution.py:239
  241.8 2.5 collective-permute-start.15
  244.3 1.3 collective-permute-start.10
  245.6 13.1 %collective-permute-done.18.rest_1_ = bf16[256,1536]{1,0:T(8,128)(2,1)S(1)} collective-permute-done((bf16[256,1536]{1,0:T(8,128)(2,1)}, bf16[256,1536]{1,0:T(8,128)(2,1)S(1)}, u32[]{:S(2)}, u32[]{:S(2)}) %collective-permute-start.18) | collective-permute-done | bytes 786464 | tf_op jit(solution)/shard_map/ppermute | solution.py:239
  258.6 0.9 copy-done.3
  259.5 1.8 collective-permute-start.16
  262.2 2.5 collective-permute-start.17
  265.6 33.9 %collective-permute-done.10.rest_7_ = bf16[256,1536]{1,0:T(8,128)(2,1)} collective-permute-done((bf16[256,1536]{1,0:T(8,128)(2,1)}, bf16[256,1536]{1,0:T(8,128)(2,1)}, u32[]{:S(2)}, u32[]{:S(2)}) %collective-permute-start.10) | collective-permute-done | bytes 786464 | tf_op jit(solution)/shard_map/ppermute | solution.py:256
  299.4 3.2 collective-permute-start.6
  302.6 19.2 %collective-permute-done.6.halo_ref = bf16[16,2048]{1,0:T(8,128)(2,1)S(1)} collective-permute-done((bf16[16,2048]{1,0:T(8,128)(2,1)S(1)}, bf16[16,2048]{1,0:T(8,128)(2,1)S(1)}, u32[]{:S(2)}, u32[]{:S(2)}) %collective-permute-start.6) | collective-permute-done | bytes 65568 | tf_op jit(solution)/shard_map/ppermute | solution.py:24
  321.8 1.6 collective-permute-start.19
  323.4 1.6 collective-permute-start.23
  325.0 1.3 collective-permute-start.24
  326.4 4.5 collective-permute-start.20
  331.6 1.9 collective-permute-start.22
  334.3 18.2 %collective-permute-done.24.rest_11_ = bf16[256,1536]{1,0:T(8,128)(2,1)} collective-permute-done((bf16[256,1536]{1,0:T(8,128)(2,1)}, bf16[256,1536]{1,0:T(8,128)(2,1)}, u32[]{:S(2)}, u32[]{:S(2)}) %collective-permute-start.24) | collective-permute-done | bytes 786464 | tf_op jit(solution)/shard_map/ppermute | solution.py:256
  352.5 2.2 collective-permute-start.26
  354.7 26.2 %shard_map.188.x_ref = bf16[1024,1536]{1,0:T(8,128)(2,1)} custom-call(bf16[1024,2048]{1,0:T(8,128)(2,1)} %all-gather.2.cloned.1.call-done.x_ref, bf16[16,2048]{1,0:T(8,128)(2,1)S(1)} %collective-permute-done.6.halo_ref, f32[6,1536]{1,0:T(8,128)S(1)} %reshape.44.taps_ref, bf16[512,1536]{1,0:T(8,128)(2,1)S(1)} %constant_dynamic-update-slice_fusion.rest_0_, ...), custom_call_target="tpu_custom_call" | custom-call | flops 12884901888 | bytes 12582912 | tf_op jit(solution)/shard_map/pallas_call | solution.py:399
  382.6 0.9 copy-done.22
  383.5 12.3 %shard_map.189 = bf16[1024,2048]{1,0:T(8,128)(2,1)} custom-call(bf16[1024,1536]{1,0:T(8,128)(2,1)} %shard_map.188.x_ref, bf16[256,1536]{1,0:T(8,128)(2,1)S(1)} %copy-done, bf16[256,1536]{1,0:T(8,128)(2,1)S(1)} %copy-done.4, bf16[256,1536]{1,0:T(8,128)(2,1)S(1)} %copy-done.2, bf16[256,1536]{1,0:T(8,128)(2,1)} %collective-permute-done.9.rest_3_, ...), custom_call_target="tpu_custom_call" | custom-call | flops 6442450944 | bytes 6291456 | tf_op jit(solution)/shard_map/pallas_call | solution.py:443
  395.9 52.9 %reduce-scatter.2.cloned.1.call-done = bf16[256,2048]{1,0:T(8,128)(2,1)} async-done(((bf16[1024,2048]{1,0:T(8,128)(2,1)}), bf16[256,2048]{1,0:T(8,128)(2,1)}) %reduce-scatter.2.cloned.1.call-update) | async-done | bytes 1048592 | tf_op jit(solution)/shard_map/reduce_scatter | solution.py:599
  448.8 2.5 add_convert_fusion
  (86 shorter events, 10.4 us)
Async XLA Ops:
  6.5 1.4 copy-start.8
  6.5 8.9 %copy-start.6 = (bf16[1024,2,256]{2,1,0:T(2,128)(2,1)S(1)}, bf16[1024,2,256]{2,1,0:T(2,128)(2,1)}, u32[]{:S(2)}) copy-start(bf16[1024,2,256]{2,1,0:T(2,128)(2,1)} %param.24) | copy-start | bytes 3145732
  6.5 258.2 %all-gather.2.cloned.1.call-start = ((), (), s32[]{:S(2)}) async-start(), calls=%async_computation.2 | async-start | bytes 5242880 | tf_op jit(solution)/shard_map/all_gather | solution.py:590
  7.9 8.7 %copy-start.14 = (f32[2,2]{1,0:T(2,128)S(1)}, f32[2,2]{1,0:T(2,128)}, u32[]{:S(2)}) copy-start(f32[2,2]{1,0:T(2,128)} %param.29) | copy-start | bytes 52
  7.9 8.7 %copy-start.10 = (f32[2,2,1024]{2,1,0:T(2,128)S(1)}, f32[2,2,1024]{2,1,0:T(2,128)}, u32[]{:S(2)}) copy-start(f32[2,2,1024]{2,1,0:T(2,128)} %param.28) | copy-start | bytes 49156
  7.9 8.7 %copy-start.11 = (f32[2,2,1024]{2,1,0:T(2,128)S(1)}, f32[2,2,1024]{2,1,0:T(2,128)}, u32[]{:S(2)}) copy-start(f32[2,2,1024]{2,1,0:T(2,128)} %param.27) | copy-start | bytes 49156
  7.9 8.7 %copy-start.12 = (bf16[2,2,1024]{2,1,0:T(2,128)(2,1)S(1)}, bf16[2,2,1024]{2,1,0:T(2,128)(2,1)}, u32[]{:S(2)}) copy-start(bf16[2,2,1024]{2,1,0:T(2,128)(2,1)} %param.26) | copy-start | bytes 24580
  7.9 8.7 %copy-start.13 = (f32[2,2]{1,0:T(2,128)S(1)}, f32[2,2]{1,0:T(2,128)}, u32[]{:S(2)}) copy-start(f32[2,2]{1,0:T(2,128)} %param.30) | copy-start | bytes 52
  8.0 45.0 %collective-permute-start = (bf16[512,1536]{1,0:T(8,128)(2,1)S(1)}, bf16[512,1536]{1,0:T(8,128)(2,1)}, u32[]{:S(2)}, u32[]{:S(2)}) collective-permute-start(bf16[512,1536]{1,0:T(8,128)(2,1)S(1)} %constant_dynamic-update-slice_fusion.rest_0_), channel_id=1, source_target_pairs={{0,8},{4,12},{8,16},{12,20},{16,24},{20,28},{1,9},{5,13},{9,17},{1... | collective-permute-start | bytes 4718600 | tf_op jit(solution)/shard_map/ppermute | solution.py:255
  14.1 38.9 %collective-permute-start.1 = (bf16[512,1536]{1,0:T(8,128)(2,1)S(1)}, bf16[512,1536]{1,0:T(8,128)(2,1)}, u32[]{:S(2)}, u32[]{:S(2)}) collective-permute-start(bf16[512,1536]{1,0:T(8,128)(2,1)S(1)} %constant_dynamic-update-slice_fusion.rest_0_), channel_id=1, source_target_pairs={{8,0},{12,4},{16,8},{20,12},{24,16},{28,20},{9,1},{13,5},{17,9},{2... | collective-permute-start | bytes 4718600 | tf_op jit(solution)/shard_map/ppermute | solution.py:256
  53.0 72.8 %collective-permute-start.2 = (bf16[512,1536]{1,0:T(8,128)(2,1)}, bf16[512,1536]{1,0:T(8,128)(2,1)}, u32[]{:S(2)}, u32[]{:S(2)}) collective-permute-start(bf16[512,1536]{1,0:T(8,128)(2,1)} %collective-permute-done.rest_2_), channel_id=1, source_target_pairs={{8,16},{12,20},{16,24},{20,28},{9,17},{13,21},{17,25},{21,29},{10,... | collective-permute-start | bytes 4718600 | tf_op jit(solution)/shard_map/ppermute | solution.py:255
  54.8 71.0 %collective-permute-start.3 = (bf16[512,1536]{1,0:T(8,128)(2,1)}, bf16[512,1536]{1,0:T(8,128)(2,1)}, u32[]{:S(2)}, u32[]{:S(2)}) collective-permute-start(bf16[512,1536]{1,0:T(8,128)(2,1)} %collective-permute-done.1.rest_3_), channel_id=1, source_target_pairs={{8,0},{12,4},{16,8},{20,12},{9,1},{13,5},{17,9},{21,13},{10,2},{14... | collective-permute-start | bytes 4718600 | tf_op jit(solution)/shard_map/ppermute | solution.py:256
  90.9 38.3 %copy-start.7 = (bf16[1024,2,256]{2,1,0:T(2,128)(2,1)S(1)}, bf16[1024,2,256]{2,1,0:T(2,128)(2,1)}, u32[]{:S(2)}) copy-start(bf16[1024,2,256]{2,1,0:T(2,128)(2,1)} %param.25) | copy-start | bytes 3145732
  125.9 39.1 %collective-permute-start.4 = (bf16[512,1536]{1,0:T(8,128)(2,1)}, bf16[512,1536]{1,0:T(8,128)(2,1)}, u32[]{:S(2)}, u32[]{:S(2)}) collective-permute-start(bf16[512,1536]{1,0:T(8,128)(2,1)} %collective-permute-done.2.rest_6_), channel_id=1, source_target_pairs={{16,24},{20,28},{17,25},{21,29},{18,26},{22,30},{19,27},{23,31}} | collective-permute-start | bytes 4718600 | tf_op jit(solution)/shard_map/ppermute | solution.py:255
  127.7 42.9 %collective-permute-start.5 = (bf16[512,1536]{1,0:T(8,128)(2,1)}, bf16[512,1536]{1,0:T(8,128)(2,1)}, u32[]{:S(2)}, u32[]{:S(2)}) collective-permute-start(bf16[512,1536]{1,0:T(8,128)(2,1)} %collective-permute-done.3.rest_7_), channel_id=1, source_target_pairs={{8,0},{12,4},{9,1},{13,5},{10,2},{14,6},{11,3},{15,7}} | collective-permute-start | bytes 4718600 | tf_op jit(solution)/shard_map/ppermute | solution.py:256
  156.8 169.5 %copy-start.9 = (bf16[3,2,1536]{2,1,0:T(2,128)(2,1)S(1)}, bf16[3,2,1536]{2,1,0:T(2,128)(2,1)}, u32[]{:S(2)}) copy-start(bf16[3,2,1536]{2,1,0:T(2,128)(2,1)} %param.36) | copy-start | bytes 55300
  170.7 278.1 %reduce-scatter.2.cloned.1.call-start = ((), (), s32[]{:S(2)}) async-start(), calls=%async_computation.3 | async-start | bytes 5242880 | tf_op jit(solution)/shard_map/reduce_scatter | solution.py:599
  170.7 37.3 %collective-permute-start.11 = (bf16[512,1536]{1,0:T(8,128)(2,1)S(1)}, bf16[512,1536]{1,0:T(8,128)(2,1)S(1)}, u32[]{:S(2)}, u32[]{:S(2)}) collective-permute-start(bf16[512,1536]{1,0:T(8,128)(2,1)S(1)} %constant_dynamic-update-slice_fusion.rest_0_), channel_id=1, source_target_pairs={{0,4},{4,0},{8,12},{12,8},{16,20},{20,16},{24,28},{28,24},{1,5},{5... | collective-permute-start | bytes 4718600 | tf_op jit(solution)/shard_map/ppermute | solution.py:239
  171.4 38.9 %collective-permute-start.12 = (bf16[512,1536]{1,0:T(8,128)(2,1)}, bf16[512,1536]{1,0:T(8,128)(2,1)S(1)}, u32[]{:S(2)}, u32[]{:S(2)}) collective-permute-start(bf16[512,1536]{1,0:T(8,128)(2,1)} %collective-permute-done.rest_2_), channel_id=1, source_target_pairs={{8,12},{12,8},{16,20},{20,16},{24,28},{28,24},{9,13},{13,9},{17,21... | collective-permute-start | bytes 4718600 | tf_op jit(solution)/shard_map/ppermute | solution.py:239
  172.1 69.6 %collective-permute-start.13 = (bf16[512,1536]{1,0:T(8,128)(2,1)}, bf16[512,1536]{1,0:T(8,128)(2,1)S(1)}, u32[]{:S(2)}, u32[]{:S(2)}) collective-permute-start(bf16[512,1536]{1,0:T(8,128)(2,1)} %collective-permute-done.1.rest_3_), channel_id=1, source_target_pairs={{0,4},{4,0},{8,12},{12,8},{16,20},{20,16},{1,5},{5,1},{9,13},{13,9... | collective-permute-start | bytes 4718600 | tf_op jit(solution)/shard_map/ppermute | solution.py:239
  175.5 33.1 %collective-permute-start.7 = (bf16[256,1536]{1,0:T(8,128)(2,1)}, bf16[256,1536]{1,0:T(8,128)(2,1)S(1)}, u32[]{:S(2)}, u32[]{:S(2)}) collective-permute-start(bf16[256,1536]{1,0:T(8,128)(2,1)} %rest_0_), channel_id=1, source_target_pairs={{0,8},{4,12},{8,16},{12,20},{16,24},{20,28},{1,9},{5,13},{9,17},{1... | collective-permute-start | bytes 2359304 | tf_op jit(solution)/shard_map/ppermute | solution.py:255
  183.9 60.4 %collective-permute-start.9 = (bf16[256,1536]{1,0:T(8,128)(2,1)}, bf16[256,1536]{1,0:T(8,128)(2,1)}, u32[]{:S(2)}, u32[]{:S(2)}) collective-permute-start(bf16[256,1536]{1,0:T(8,128)(2,1)} %rest_0_), channel_id=1, source_target_pairs={{8,0},{12,4},{16,8},{20,12},{24,16},{28,20},{9,1},{13,5},{17,9},{2... | collective-permute-start | bytes 2359304 | tf_op jit(solution)/shard_map/ppermute | solution.py:256
  208.1 50.6 %collective-permute-start.18 = (bf16[256,1536]{1,0:T(8,128)(2,1)}, bf16[256,1536]{1,0:T(8,128)(2,1)S(1)}, u32[]{:S(2)}, u32[]{:S(2)}) collective-permute-start(bf16[256,1536]{1,0:T(8,128)(2,1)} %rest_0_), channel_id=1, source_target_pairs={{0,4},{4,0},{8,12},{12,8},{16,20},{20,16},{24,28},{28,24},{1,5},{5... | collective-permute-start | bytes 2359304 | tf_op jit(solution)/shard_map/ppermute | solution.py:239
  208.6 0.9 copy-start.1
  209.5 51.8 %collective-permute-start.8 = (bf16[256,1536]{1,0:T(8,128)(2,1)S(1)}, bf16[256,1536]{1,0:T(8,128)(2,1)S(1)}, u32[]{:S(2)}, u32[]{:S(2)}) collective-permute-start(bf16[256,1536]{1,0:T(8,128)(2,1)S(1)} %collective-permute-done.7.rest_2_), channel_id=1, source_target_pairs={{8,16},{12,20},{16,24},{20,28},{9,17},{13,21},{17,25},{21,29},{10,... | collective-permute-start | bytes 2359304 | tf_op jit(solution)/shard_map/ppermute | solution.py:255
  210.3 51.1 %copy-start.15 = (bf16[512,1536]{1,0:T(8,128)(2,1)}, bf16[512,1536]{1,0:T(8,128)(2,1)S(1)}, u32[]{:S(2)}) copy-start(bf16[512,1536]{1,0:T(8,128)(2,1)S(1)} %collective-permute-done.12.rest_4_) | copy-start | bytes 4718596
  210.3 113.1 %collective-permute-start.14 = (bf16[512,1536]{1,0:T(8,128)(2,1)}, bf16[512,1536]{1,0:T(8,128)(2,1)}, u32[]{:S(2)}, u32[]{:S(2)}) collective-permute-start(bf16[512,1536]{1,0:T(8,128)(2,1)} %collective-permute-done.2.rest_6_), channel_id=1, source_target_pairs={{16,20},{20,16},{24,28},{28,24},{17,21},{21,17},{25,29},{29,25},{1... | collective-permute-start | bytes 4718600 | tf_op jit(solution)/shard_map/ppermute | solution.py:239
  241.8 19.6 %copy-start.16 = (bf16[512,1536]{1,0:T(8,128)(2,1)}, bf16[512,1536]{1,0:T(8,128)(2,1)S(1)}, u32[]{:S(2)}) copy-start(bf16[512,1536]{1,0:T(8,128)(2,1)S(1)} %collective-permute-done.13.rest_5_) | copy-start | bytes 4718596
  241.8 83.2 %collective-permute-start.15 = (bf16[512,1536]{1,0:T(8,128)(2,1)}, bf16[512,1536]{1,0:T(8,128)(2,1)}, u32[]{:S(2)}, u32[]{:S(2)}) collective-permute-start(bf16[512,1536]{1,0:T(8,128)(2,1)} %collective-permute-done.3.rest_7_), channel_id=1, source_target_pairs={{0,4},{4,0},{8,12},{12,8},{1,5},{5,1},{9,13},{13,9},{2,6},{6,2},{1... | collective-permute-start | bytes 4718600 | tf_op jit(solution)/shard_map/ppermute | solution.py:239
  244.3 55.2 %collective-permute-start.10 = (bf16[256,1536]{1,0:T(8,128)(2,1)}, bf16[256,1536]{1,0:T(8,128)(2,1)}, u32[]{:S(2)}, u32[]{:S(2)}) collective-permute-start(bf16[256,1536]{1,0:T(8,128)(2,1)} %collective-permute-done.9.rest_3_), channel_id=1, source_target_pairs={{8,0},{12,4},{16,8},{20,12},{9,1},{13,5},{17,9},{21,13},{10,2},{14... | collective-permute-start | bytes 2359304 | tf_op jit(solution)/shard_map/ppermute | solution.py:256
  259.5 71.4 %collective-permute-start.16 = (bf16[512,1536]{1,0:T(8,128)(2,1)}, bf16[512,1536]{1,0:T(8,128)(2,1)}, u32[]{:S(2)}, u32[]{:S(2)}) collective-permute-start(bf16[512,1536]{1,0:T(8,128)(2,1)} %collective-permute-done.4.rest_10_), channel_id=1, source_target_pairs={{24,28},{28,24},{25,29},{29,25},{26,30},{30,26},{27,31},{31,27}} | collective-permute-start | bytes 4718600 | tf_op jit(solution)/shard_map/ppermute | solution.py:239
  262.2 69.4 %collective-permute-start.17 = (bf16[512,1536]{1,0:T(8,128)(2,1)}, bf16[512,1536]{1,0:T(8,128)(2,1)}, u32[]{:S(2)}, u32[]{:S(2)}) collective-permute-start(bf16[512,1536]{1,0:T(8,128)(2,1)} %collective-permute-done.5.rest_11_), channel_id=1, source_target_pairs={{0,4},{4,0},{1,5},{5,1},{2,6},{6,2},{3,7},{7,3}} | collective-permute-start | bytes 4718600 | tf_op jit(solution)/shard_map/ppermute | solution.py:239
  299.4 22.4 %collective-permute-start.6 = (bf16[16,2048]{1,0:T(8,128)(2,1)S(1)}, bf16[16,2048]{1,0:T(8,128)(2,1)S(1)}, u32[]{:S(2)}, u32[]{:S(2)}) collective-permute-start(bf16[16,2048]{1,0:T(8,128)(2,1)S(1)} %slice.4), channel_id=1, source_target_pairs={{0,4},{4,8},{8,12},{12,16},{16,20},{20,24},{24,28},{1,5},{5,9},{9,... | collective-permute-start | bytes 196616 | tf_op jit(solution)/shard_map/ppermute | solution.py:24
  321.8 4.5 collective-permute-start.19
  323.4 10.1 %collective-permute-start.23 = (bf16[256,1536]{1,0:T(8,128)(2,1)}, bf16[256,1536]{1,0:T(8,128)(2,1)}, u32[]{:S(2)}, u32[]{:S(2)}) collective-permute-start(bf16[256,1536]{1,0:T(8,128)(2,1)} %copy-done.17), channel_id=1, source_target_pairs={{16,24},{20,28},{17,25},{21,29},{18,26},{22,30},{19,27},{23,31}} | collective-permute-start | bytes 2359304 | tf_op jit(solution)/shard_map/ppermute | solution.py:255
  325.0 27.5 %collective-permute-start.24 = (bf16[256,1536]{1,0:T(8,128)(2,1)}, bf16[256,1536]{1,0:T(8,128)(2,1)}, u32[]{:S(2)}, u32[]{:S(2)}) collective-permute-start(bf16[256,1536]{1,0:T(8,128)(2,1)} %collective-permute-done.10.rest_7_), channel_id=1, source_target_pairs={{8,0},{12,4},{9,1},{13,5},{10,2},{14,6},{11,3},{15,7}} | collective-permute-start | bytes 2359304 | tf_op jit(solution)/shard_map/ppermute | solution.py:256
  326.3 57.2 %copy-start = (bf16[256,1536]{1,0:T(8,128)(2,1)S(1)}, bf16[256,1536]{1,0:T(8,128)(2,1)}, u32[]{:S(2)}) copy-start(bf16[256,1536]{1,0:T(8,128)(2,1)} %rest_0_) | copy-start | bytes 2359300
  326.3 57.2 %copy-start.2 = (bf16[256,1536]{1,0:T(8,128)(2,1)S(1)}, bf16[256,1536]{1,0:T(8,128)(2,1)}, u32[]{:S(2)}) copy-start(bf16[256,1536]{1,0:T(8,128)(2,1)} %copy-done.1) | copy-start | bytes 2359300
  326.3 57.2 %copy-start.4 = (bf16[256,1536]{1,0:T(8,128)(2,1)S(1)}, bf16[256,1536]{1,0:T(8,128)(2,1)}, u32[]{:S(2)}) copy-start(bf16[256,1536]{1,0:T(8,128)(2,1)} %copy-done.3) | copy-start | bytes 2359300
  326.4 54.5 %collective-permute-start.20 = (bf16[256,1536]{1,0:T(8,128)(2,1)}, bf16[256,1536]{1,0:T(8,128)(2,1)S(1)}, u32[]{:S(2)}, u32[]{:S(2)}) collective-permute-start(bf16[256,1536]{1,0:T(8,128)(2,1)} %collective-permute-done.9.rest_3_), channel_id=1, source_target_pairs={{0,4},{4,0},{8,12},{12,8},{16,20},{20,16},{1,5},{5,1},{9,13},{13,9... | collective-permute-start | bytes 2359304 | tf_op jit(solution)/shard_map/ppermute | solution.py:239
  330.9 50.0 %collective-permute-start.21 = (bf16[256,1536]{1,0:T(8,128)(2,1)}, bf16[256,1536]{1,0:T(8,128)(2,1)S(1)}, u32[]{:S(2)}, u32[]{:S(2)}) collective-permute-start(bf16[256,1536]{1,0:T(8,128)(2,1)} %copy-done.17), channel_id=1, source_target_pairs={{16,20},{20,16},{24,28},{28,24},{17,21},{21,17},{25,29},{29,25},{1... | collective-permute-start | bytes 2359304 | tf_op jit(solution)/shard_map/ppermute | solution.py:239
  331.6 49.3 %collective-permute-start.22 = (bf16[256,1536]{1,0:T(8,128)(2,1)}, bf16[256,1536]{1,0:T(8,128)(2,1)S(1)}, u32[]{:S(2)}, u32[]{:S(2)}) collective-permute-start(bf16[256,1536]{1,0:T(8,128)(2,1)} %collective-permute-done.10.rest_7_), channel_id=1, source_target_pairs={{0,4},{4,0},{8,12},{12,8},{1,5},{5,1},{9,13},{13,9},{2,6},{6,2},{1... | collective-permute-start | bytes 2359304 | tf_op jit(solution)/shard_map/ppermute | solution.py:239
  333.6 47.4 %collective-permute-start.25 = (bf16[256,1536]{1,0:T(8,128)(2,1)}, bf16[256,1536]{1,0:T(8,128)(2,1)S(1)}, u32[]{:S(2)}, u32[]{:S(2)}) collective-permute-start(bf16[256,1536]{1,0:T(8,128)(2,1)} %collective-permute-done.23.rest_10_), channel_id=1, source_target_pairs={{24,28},{28,24},{25,29},{29,25},{26,30},{30,26},{27,31},{31,27}} | collective-permute-start | bytes 2359304 | tf_op jit(solution)/shard_map/ppermute | solution.py:239
  352.5 28.5 %collective-permute-start.26 = (bf16[256,1536]{1,0:T(8,128)(2,1)}, bf16[256,1536]{1,0:T(8,128)(2,1)S(1)}, u32[]{:S(2)}, u32[]{:S(2)}) collective-permute-start(bf16[256,1536]{1,0:T(8,128)(2,1)} %collective-permute-done.24.rest_11_), channel_id=1, source_target_pairs={{0,4},{4,0},{1,5},{5,1},{2,6},{6,2},{3,7},{7,3}} | collective-permute-start | bytes 2359304 | tf_op jit(solution)/shard_map/ppermute | solution.py:239
  380.9 1.1 copy-start.19
  380.9 1.4 copy-start.20
  381.0 1.7 copy-start.21
  395.9 53.0 %copy-start.5 = (f32[256,2048]{1,0:T(8,128)S(1)}, f32[256,2048]{1,0:T(8,128)}, u32[]{:S(2)}) copy-start(f32[256,2048]{1,0:T(8,128)} %get-tuple-element.48) | copy-start | bytes 6291460
  (4 other events, 3.5 us)
Sparse Core Ops, SparseCore 0:
  170.8 40.2 all-gather.1
  396.0 52.7 reduce-scatter.1
where the time goes:
time: 459 us; the launch traced here: 458 us
  waiting for transfers between devices  196 us (43%)
  Pallas kernels  157 us (34%)
  starting transfers between devices  57 us (12%)
  blocking collectives  17 us (4%)
  local copies, waits for them, and re-layouts  15.2 us (3%)
  between operations  14 us (3%)
    pallas_call x4, Pallas kernels, local_terms(): pl.pallas_call(local_kernel, grid=(steps,), in_specs=[pl.BlockSpec((CHUNK...  69.4 us
    ppermute x14, waiting for transfers between devices, swapped(): return lax.ppermute(value, 'sp', [(i, i ^ 1) for i in places])  65.7 us
    ppermute x6, waiting for transfers between devices, line_step(): left = lax.ppermute(line['left'], 'sp', down)  57.8 us
    reduce_scatter x1, waiting for transfers between devices, per_device(): lax.psum_scatter(down_part(hidden, features.shape[1], down['pieces']), 't...  52.9 us
    pallas_call x1, Pallas kernels, exchange(): pl.pallas_call(exchange_kernel, in_specs=[pl.BlockSpec(memory_space=pltpu...  35 us
    pallas_call x1, Pallas kernels, up_part(): pl.pallas_call(functools.partial(up_kernel, meta), grid=(length // tile,)...  26.2 us
    ppermute x14, starting transfers between devices, swapped(): return lax.ppermute(value, 'sp', [(i, i ^ 1) for i in places])  25.5 us
    ppermute x6, starting transfers between devices, line_step(): right = lax.ppermute(line['right'], 'sp', up)  20.4 us
  transfers between devices with their start and end apart: 29, of which 8 were waited for; matrix products, arithmetic and copies ran while one was open for 2% of the time, Pallas kernels for 31%

commit v1 on v0

--- a/solution.py
+++ b/solution.py
@@ -320,7 +320,7 @@
     def _():
         sum_ref[...] = skip_ref[...].astype(F32)
 
-    sum_ref[...] += jnp.dot(x_ref[...], w_ref[...], preferred_element_type=F32)
+    sum_ref[...] += jnp.dot(x_ref[0], w_ref[...], preferred_element_type=F32)
 
     @pl.when(step == pl.num_programs(0) - 1)
     def _():
@@ -330,16 +330,16 @@
 
 
 def project(x, weights, skip, coef):
-    rows, depth = x.shape
-    width = weights.shape[1]
-    part = min(512, depth)
+    team, rows, wide = x.shape
+    depth, width = weights.shape
+    part = wide // 2
     whole = pl.BlockSpec((rows, width), lambda i: (0, 0))
     return pl.pallas_call(
         project_kernel,
         grid=(depth // part,),
         in_specs=[
-            pl.BlockSpec((rows, part), lambda i: (0, i)),
-            pl.BlockSpec((part, width), lambda i: (i, 0)),
+            pl.BlockSpec((1, rows, part), lambda i: (i // 2, 0, i % 2)),
+            pl.BlockSpec((part, width), lambda i: ((i % 2) * team + i // 2, 0)),
             whole,
             pl.BlockSpec((1, width), lambda i: (0, 0)),
         ],
@@ -426,7 +426,7 @@
 
     @pl.when(pl.program_id(0) == 0)
     def _():
-        copies = load_pieces(meta, refs, ((0, rows),), (down_w,), sem)
+        copies = load_pieces(meta, refs, ((2 * rows, 3 * rows),), (down_w,), sem)
         finish_pieces(copies)
 
     wide = out_ref.shape[1]
@@ -540,7 +540,9 @@
     gates_beta = jnp.concatenate([level, beta_rate], axis=0).reshape(-1, length)
     gates_beta = jnp.pad(gates_beta, ((0, -gates_beta.shape[0] % 8), (0, 0)))
     spare = -latter_request_vectors.shape[1] % LANES
-    sides = jnp.concatenate([switching_channel_map, broadening_channel_map], axis=0)
+    sides = jnp.concatenate(
+        [switching_channel_map, broadening_channel_map, narrowing_map_weights_in], axis=0
+    )
     side = line_step(line_start(sides), 1)
     units = former_request_vectors.shape[1] // LANES + (
         latter_request_vectors.shape[1] + spare
@@ -558,15 +560,14 @@
     done = ()
     summary = None
     for part in range(parts):
-        if part == parts // 2:
+        if part == parts - 1:
             side, running = tie(side, running)
             side = line_step(line_swap(side, 1), 2)
         *done, running, summary = local_terms(*drawn, running, part, parts, tuple(done))
     g_part, h_part = done
     everyone = exchange(summary)
-    side, (everyone, narrow) = tie(side, (everyone, narrowing_map_weights_in))
+    side, everyone = tie(side, everyone)
     side = line_step(line_swap(side, 2), 3)
-    down = line_step(line_start(narrow), 1)
     place = lax.axis_index("sp").astype(jnp.int32).reshape(1)
     attended = finish_heads(
         place,
@@ -576,11 +577,12 @@
         closing_valve_operands.reshape(length, -1),
         unitwise_normalizer_coef.reshape(1, -1),
     )
-    linear_attend = attended.reshape(length, 2, -1)
-    arrived = lax.all_to_all(linear_attend, "tp", split_axis=0, concat_axis=2, tiled=True)
-    row_count = arrived.shape[0]
+    team = lax.axis_size("tp")
+    arrived = lax.all_to_all(
+        attended.reshape(team, length // team, -1), "tp", split_axis=0, concat_axis=0, tiled=True
+    )
     skip_stream, normed = project(
-        arrived.reshape(row_count, -1),
+        arrived,
         emission_map_weights,
         arriving_hidden_state,
         channel_normalizer_coef.reshape(1, -1),
@@ -588,21 +590,32 @@
     side, normed = tie(side, normed)
     side = line_rest(line_swap(side, 3), 4)
     features = lax.all_gather(normed, "tp", axis=0, tiled=True)
-    down = line_step(line_swap(down, 1), 2)
     edge = 16
     halo = from_behind(features[-edge:], "sp", 1)
     taps = timewise_convolve_tapvalues.astype(F32).reshape(2 * TAPS, -1)
-    down, halo = tie(down, halo)
-    down = line_step(line_swap(down, 2), 3)
     hidden = up_part(features, halo, taps, side["pieces"])
-    down = line_rest(line_swap(down, 3), 4)
-    down_sum = lax.psum_scatter(
-        down_part(hidden, features.shape[1], down["pieces"]),
-        "tp",
-        scatter_dimension=0,
-        tiled=True,
-    ).astype(jnp.float32)
-    return (skip_stream + down_sum).astype(jnp.bfloat16)
+    partial = down_part(hidden, features.shape[1], side["pieces"])
+    return (skip_stream + team_sum(partial)).astype(jnp.bfloat16)
+
+
+def team_sum(partial):
+    team = lax.axis_size("tp")
+    if team != 4:
+        return lax.psum_scatter(partial, "tp", scatter_dimension=0, tiled=True).astype(F32)
+    me = lax.axis_index("tp")
+    core, place = me % 2, me // 2
+    blocks = partial.reshape(2, 2, -1, partial.shape[1])
+    away = lax.dynamic_index_in_dim(blocks, 1 - core, 1, False)
+    came = lax.ppermute(away, "tp", [(i, i ^ 1) for i in range(team)])
+    mine = lax.dynamic_index_in_dim(blocks, core, 1, False)
+
+    def both(which):
+        return lax.dynamic_index_in_dim(mine, which, 0, False).astype(F32) + (
+            lax.dynamic_index_in_dim(came, which, 0, False).astype(F32)
+        )
+
+    across = lax.ppermute(both(1 - place).astype(BF16), "tp", [(i, i ^ 2) for i in range(team)])
+    return both(place) + across.astype(F32)
 
 
 def solution(mesh):

time: 459 us -> 504 us (1.098)
  waiting for transfers between devices: 196 us -> 257 us
  starting transfers between devices: 57 us -> 36.8 us
    ppermute x14 -> x7, waiting for transfers between devices: 65.7 us -> 180 us  [swapped(): return lax.ppermute(value, 'sp', [(i, i ^ 1) for i in places])]
    reduce_scatter x1 -> x0, waiting for transfers between devices: 52.9 us -> none  [per_device(): lax.psum_scatter(down_part(hidden, features.shape[1], down['pieces']), 't...]
    ppermute x0 -> x2, waiting for transfers between devices: none -> 28.3 us  [the longest x1 23.8 us: team_sum(): lax.ppermute(both(1 - place).astype(BF16), 'tp', [(i, i ^ 2) for i in ran...]
    ppermute x1, waiting for transfers between devices: 19.2 us -> 0.34 us  [from_behind(): lax.ppermute(value, axis, [(source, source + steps) for source in range(l...]
    ppermute x6 -> x3, starting transfers between devices: 20.4 us -> 10.6 us  [line_step(): right = lax.ppermute(line['right'], 'sp', up)]
    ppermute x6 -> x3, waiting for transfers between devices: 57.8 us -> 48.5 us  [line_step(): left = lax.ppermute(line['left'], 'sp', down)]
    ppermute x14 -> x7, starting transfers between devices: 25.5 us -> 17.1 us  [swapped(): return lax.ppermute(value, 'sp', [(i, i ^ 1) for i in places])]
  transfers between devices with their start and end apart: 29 -> 17, of which waited for: 8 -> 9; matrix products, arithmetic and copies ran while one was open for 2% -> 1% of each run, Pallas kernels for 31% -> 24%
where the time goes in v1:
time: 504 us; the launch traced here: 503 us
  waiting for transfers between devices  257 us (51%)
  Pallas kernels  159 us (32%)
  starting transfers between devices  36.8 us (7%)
  blocking collectives  18.7 us (4%)
  between operations  13.7 us (3%)
  local copies, waits for them, and re-layouts  11.9 us (2%)
  other arithmetic  5.61 us (1%)
    ppermute x7, waiting for transfers between devices, swapped(): return lax.ppermute(value, 'sp', [(i, i ^ 1) for i in places])  180 us
    pallas_call x4, Pallas kernels, local_terms(): pl.pallas_call(local_kernel, grid=(steps,), in_specs=[pl.BlockSpec((CHUNK...  69.5 us
    ppermute x3, waiting for transfers between devices, line_step(): left = lax.ppermute(line['left'], 'sp', down)  48.5 us
    pallas_call x1, Pallas kernels, exchange(): pl.pallas_call(exchange_kernel, in_specs=[pl.BlockSpec(memory_space=pltpu...  34.9 us
    pallas_call x1, Pallas kernels, up_part(): pl.pallas_call(functools.partial(up_kernel, meta), grid=(length // tile,)...  26.5 us
    ppermute x1, waiting for transfers between devices, team_sum(): lax.ppermute(both(1 - place).astype(BF16), 'tp', [(i, i ^ 2) for i in ran...  23.8 us
    all_to_all x1, blocking collectives, per_device(): lax.all_to_all(attended.reshape(team, length // team, -1), 'tp', split_ax...  18.7 us
    ppermute x7, starting transfers between devices, swapped(): return lax.ppermute(value, 'sp', [(i, i ^ 1) for i in places])  17.1 us
  transfers between devices with their start and end apart: 17, of which 9 were waited for; matrix products, arithmetic and copies ran while one was open for 1% of the time, Pallas kernels for 24%

profile of v1, /device:TPU:0, one launch (start us, length us, event | category | flops | bytes accessed | tf_op | source)
XLA Modules:
  0.0 503.0 jit_solution(12044723580966837631)
XLA Ops:
  6.6 1.3 constant_dynamic-update-slice_fusion.2
  7.9 1.2 constant_dynamic-update-slice_fusion.1
  9.1 0.1 constant_dynamic-update-slice_fusion.rest_0_
  9.2 6.4 %collective-permute-start = (bf16[768,1536]{1,0:T(8,128)(2,1)S(1)}, bf16[768,1536]{1,0:T(8,128)(2,1)}, u32[]{:S(2)}, u32[]{:S(2)}) collective-permute-start(bf16[768,1536]{1,0:T(8,128)(2,1)S(1)} %constant_dynamic-update-slice_fusion.rest_0_), channel_id=1, source_target_pairs={{0,8},{4,12},{8,16},{12,20},{16,24},{20,28},{1,9},{5,13},{9,17},{1... | collective-permute-start | bytes 7077896 | tf_op jit(solution)/shard_map/ppermute | solution.py:255
  15.6 1.3 collective-permute-start.1
  17.0 0.1 fusion.6
  17.1 1.2 copy.26
  18.3 0.6 reshape.46.gb_ref
  19.0 0.1 fusion.4
  19.1 0.8 broadcast_in_dim.2.from_ref
  19.9 17.4 %shard_map.181 = (bf16[1024,512]{1,0:T(8,128)(2,1)}, f32[1024,512]{1,0:T(8,128)}, f32[3,128,256]{2,1,0:T(8,128)}, bf16[3,128,256]{2,1,0:T(8,128)(2,1)}) custom-call(bf16[1024,256]{1,0:T(8,128)(2,1)} %q1_ref.7, bf16[1024,256]{1,0:T(8,128)(2,1)} %k1_ref.7, bf16[1024,128]{1,0:T(8,128)(2,1)} %q2_ref.7, bf16[1024,128]{1,0:T(8,128)(2,1)} %k2_ref.7, ...), custom_call_target="tpu_custom_call" | custom-call | flops 6710886400 | bytes 5242880 | tf_op jit(solution)/shard_map/pallas_call | solution.py:152
  37.2 17.4 %shard_map.182 = (bf16[1024,512]{1,0:T(8,128)(2,1)}, f32[1024,512]{1,0:T(8,128)}, f32[3,128,256]{2,1,0:T(8,128)}, bf16[3,128,256]{2,1,0:T(8,128)(2,1)}) custom-call(bf16[1024,256]{1,0:T(8,128)(2,1)} %q1_ref.7, bf16[1024,256]{1,0:T(8,128)(2,1)} %k1_ref.7, bf16[1024,128]{1,0:T(8,128)(2,1)} %q2_ref.7, ...), custom_call_target="tpu_custom_call", output_to_operand_aliasing={{0}: (7, {}), {1}: (8, {})} | custom-call | flops 6710886400 | bytes 5242880 | tf_op jit(solution)/shard_map/pallas_call | solution.py:152
  54.6 17.4 %shard_map.183 = (bf16[1024,512]{1,0:T(8,128)(2,1)}, f32[1024,512]{1,0:T(8,128)}, f32[3,128,256]{2,1,0:T(8,128)}, bf16[3,128,256]{2,1,0:T(8,128)(2,1)}) custom-call(bf16[1024,256]{1,0:T(8,128)(2,1)} %q1_ref.7, bf16[1024,256]{1,0:T(8,128)(2,1)} %k1_ref.7, bf16[1024,128]{1,0:T(8,128)(2,1)} %q2_ref.7, ...), custom_call_target="tpu_custom_call", output_to_operand_aliasing={{0}: (7, {}), {1}: (8, {})} | custom-call | flops 6710886400 | bytes 5242880 | tf_op jit(solution)/shard_map/pallas_call | solution.py:152
  72.0 2.1 collective-permute-start.2
  74.2 1.3 collective-permute-start.3
  75.4 17.4 %shard_map.184 = (bf16[1024,512]{1,0:T(8,128)(2,1)}, f32[1024,512]{1,0:T(8,128)}, f32[3,128,256]{2,1,0:T(8,128)}, bf16[3,128,256]{2,1,0:T(8,128)(2,1)}) custom-call(bf16[1024,256]{1,0:T(8,128)(2,1)} %q1_ref.7, bf16[1024,256]{1,0:T(8,128)(2,1)} %k1_ref.7, bf16[1024,128]{1,0:T(8,128)(2,1)} %q2_ref.7, ...), custom_call_target="tpu_custom_call", output_to_operand_aliasing={{0}: (7, {}), {1}: (8, {})} | custom-call | flops 6710886400 | bytes 5242880 | tf_op jit(solution)/shard_map/pallas_call | solution.py:152
  92.8 34.9 %shard_map.185.all_ref = bf16[8,3,128,256]{3,2,1,0:T(8,128)(2,1)} custom-call(bf16[3,128,256]{2,1,0:T(8,128)(2,1)} %get-tuple-element.38.own_ref), custom_call_target="tpu_custom_call" | custom-call | flops 1000000000 | bytes 1000000 | tf_op jit(solution)/shard_map/pallas_call | solution.py:226
  127.8 3.0 collective-permute-done.3.rest_7_
  130.8 2.1 collective-permute-start.4
  132.8 1.5 collective-permute-start.5
  134.3 1.2 copy.27
  135.5 5.5 %shard_map.186 = bf16[1024,512]{1,0:T(8,128)(2,1)} custom-call(s32[1]{0:T(128)} %bitcast.place_ref, bf16[8,3,128,256]{3,2,1,0:T(8,128)(2,1)} %shard_map.185.all_ref, bf16[1024,512]{1,0:T(8,128)(2,1)} %get-tuple-element.42.g_ref, f32[1024,512]{1,0:T(8,128)} %get-tuple-element.43.h_ref, bf16[1024,512]{1,0:T(8,128)(2,1)} %bitcast.26, f32[1,128]{1,0:T(1,128)} %bitcast.35), custom_call_target="tpu_custom_call" | custom-call | flops 1073741824 | bytes 5242880 | tf_op jit(solution)/shard_map/pallas_call | solution.py:490
  141.0 18.7 %all_to_all.5.x_ref = bf16[4,256,512]{2,1,0:T(8,128)(2,1)} all-to-all(bf16[4,256,512]{2,1,0:T(8,128)(2,1)} %bitcast.27), channel_id=1, replica_groups=mesh['sp'=8,'tp'=4] {'tp'}, dimensions={0} | all-to-all | bytes 2097152 | tf_op jit(solution)/shard_map/all_to_all | solution.py:581
  159.7 10.1 %shard_map.187 = (f32[256,2048]{1,0:T(8,128)}, bf16[256,2048]{1,0:T(8,128)(2,1)}) custom-call(bf16[4,256,512]{2,1,0:T(8,128)(2,1)} %all_to_all.5.x_ref, bf16[2048,2048]{1,0:T(8,128)(2,1)} %w_ref.1, bf16[256,2048]{1,0:T(8,128)(2,1)} %skip_ref.1, f32[1,2048]{1,0:T(1,128)} %bitcast.34), custom_call_target="tpu_custom_call" | custom-call | flops 2147483648 | bytes 8388608 | tf_op jit(solution)/shard_map/pallas_call | solution.py:337
  169.9 45.5 %collective-permute-done.5.rest_11_ = bf16[768,1536]{1,0:T(8,128)(2,1)} collective-permute-done((bf16[768,1536]{1,0:T(8,128)(2,1)}, bf16[768,1536]{1,0:T(8,128)(2,1)}, u32[]{:S(2)}, u32[]{:S(2)}) %collective-permute-start.5) | collective-permute-done | bytes 2359328 | tf_op jit(solution)/shard_map/ppermute | solution.py:256
  215.4 1.6 collective-permute-start.7
  217.0 2.1 collective-permute-start.8
  219.1 2.4 collective-permute-start.9
  221.5 2.1 collective-permute-start.10
  223.7 3.4 collective-permute-start.11
  227.1 42.5 %collective-permute-done.7.rest_1_ = bf16[768,1536]{1,0:T(8,128)(2,1)S(1)} collective-permute-done((bf16[768,1536]{1,0:T(8,128)(2,1)S(1)}, bf16[768,1536]{1,0:T(8,128)(2,1)S(1)}, u32[]{:S(2)}, u32[]{:S(2)}) %collective-permute-start.7) | collective-permute-done | bytes 2359328 | tf_op jit(solution)/shard_map/ppermute | solution.py:239
  269.6 1.4 copy-done
  271.0 2.0 collective-permute-start.12
  273.1 3.4 collective-permute-start.13
  276.5 0.8 slice.4
  277.4 42.9 %collective-permute-done.9.rest_5_ = bf16[768,1536]{1,0:T(8,128)(2,1)} collective-permute-done((bf16[768,1536]{1,0:T(8,128)(2,1)}, bf16[768,1536]{1,0:T(8,128)(2,1)}, u32[]{:S(2)}, u32[]{:S(2)}) %collective-permute-start.9) | collective-permute-done | bytes 2359328 | tf_op jit(solution)/shard_map/ppermute | solution.py:239
  320.3 3.4 collective-permute-start.6
  323.7 47.1 %collective-permute-done.11.rest_9_ = bf16[768,1536]{1,0:T(8,128)(2,1)} collective-permute-done((bf16[768,1536]{1,0:T(8,128)(2,1)}, bf16[768,1536]{1,0:T(8,128)(2,1)}, u32[]{:S(2)}, u32[]{:S(2)}) %collective-permute-start.11) | collective-permute-done | bytes 2359328 | tf_op jit(solution)/shard_map/ppermute | solution.py:239
  370.8 47.4 %collective-permute-done.13.rest_13_ = bf16[768,1536]{1,0:T(8,128)(2,1)} collective-permute-done((bf16[768,1536]{1,0:T(8,128)(2,1)}, bf16[768,1536]{1,0:T(8,128)(2,1)}, u32[]{:S(2)}, u32[]{:S(2)}) %collective-permute-start.13) | collective-permute-done | bytes 2359328 | tf_op jit(solution)/shard_map/ppermute | solution.py:239
  418.2 0.3 collective-permute-done.6.halo_ref
  418.6 26.5 %shard_map.188.x_ref = bf16[1024,1536]{1,0:T(8,128)(2,1)} custom-call(bf16[1024,2048]{1,0:T(8,128)(2,1)} %all-gather.2.cloned.1.call-done.x_ref, bf16[16,2048]{1,0:T(8,128)(2,1)S(1)} %collective-permute-done.6.halo_ref, f32[6,1536]{1,0:T(8,128)S(1)} %reshape.55.taps_ref, bf16[768,1536]{1,0:T(8,128)(2,1)S(1)} %constant_dynamic-update-slice_fusion.rest_0_, ...), custom_call_target="tpu_custom_call" | custom-call | flops 12884901888 | bytes 12582912 | tf_op jit(solution)/shard_map/pallas_call | solution.py:399
  445.1 12.5 %shard_map.189 = bf16[1024,2048]{1,0:T(8,128)(2,1)} custom-call(bf16[1024,1536]{1,0:T(8,128)(2,1)} %shard_map.188.x_ref, bf16[768,1536]{1,0:T(8,128)(2,1)S(1)} %constant_dynamic-update-slice_fusion.rest_0_, bf16[768,1536]{1,0:T(8,128)(2,1)} %copy-done, bf16[768,1536]{1,0:T(8,128)(2,1)} %collective-permute-done.rest_2_, ...), custom_call_target="tpu_custom_call" | custom-call | flops 6442450944 | bytes 6291456 | tf_op jit(solution)/shard_map/pallas_call | solution.py:443
  457.6 3.2 dynamic-slice_bitcast_fusion
  460.9 4.5 collective-permute-done.14
  465.4 1.9 fusion
  467.3 1.6 collective-permute-start.15
  468.9 23.8 %collective-permute-done.15 = bf16[256,2048]{1,0:T(8,128)(2,1)} collective-permute-done((bf16[256,2048]{1,0:T(8,128)(2,1)S(1)}, bf16[256,2048]{1,0:T(8,128)(2,1)}, u32[]{:S(2)}, u32[]{:S(2)}) %collective-permute-start.15) | collective-permute-done | bytes 1048608 | tf_op jit(solution)/shard_map/ppermute | solution.py:617
  492.7 3.5 fusion.3
  (36 shorter events, 0.2 us)
Async XLA Ops:
  6.5 10.4 %copy-start.10 = (f32[2,2]{1,0:T(2,128)S(1)}, f32[2,2]{1,0:T(2,128)}, u32[]{:S(2)}) copy-start(f32[2,2]{1,0:T(2,128)} %param.29) | copy-start | bytes 52
  6.5 10.4 %copy-start.6 = (f32[2,2,1024]{2,1,0:T(2,128)S(1)}, f32[2,2,1024]{2,1,0:T(2,128)}, u32[]{:S(2)}) copy-start(f32[2,2,1024]{2,1,0:T(2,128)} %param.28) | copy-start | bytes 49156
  6.5 10.4 %copy-start.7 = (f32[2,2,1024]{2,1,0:T(2,128)S(1)}, f32[2,2,1024]{2,1,0:T(2,128)}, u32[]{:S(2)}) copy-start(f32[2,2,1024]{2,1,0:T(2,128)} %param.27) | copy-start | bytes 49156
  6.5 10.4 %copy-start.9 = (f32[2,2]{1,0:T(2,128)S(1)}, f32[2,2]{1,0:T(2,128)}, u32[]{:S(2)}) copy-start(f32[2,2]{1,0:T(2,128)} %param.30) | copy-start | bytes 52
  6.5 10.4 %copy-start.8 = (bf16[2,2,1024]{2,1,0:T(2,128)(2,1)S(1)}, bf16[2,2,1024]{2,1,0:T(2,128)(2,1)}, u32[]{:S(2)}) copy-start(bf16[2,2,1024]{2,1,0:T(2,128)(2,1)} %param.26) | copy-start | bytes 24580
  6.5 10.6 %copy-start.2 = (bf16[1024,2,256]{2,1,0:T(2,128)(2,1)S(1)}, bf16[1024,2,256]{2,1,0:T(2,128)(2,1)}, u32[]{:S(2)}) copy-start(bf16[1024,2,256]{2,1,0:T(2,128)(2,1)} %param.24) | copy-start | bytes 3145732
  6.6 270.0 %all-gather.2.cloned.1.call-start = ((), (), s32[]{:S(2)}) async-start(), calls=%async_computation.1 | async-start | bytes 5242880 | tf_op jit(solution)/shard_map/all_gather | solution.py:592
  6.6 2.5 copy-start.4
  9.2 62.8 %collective-permute-start = (bf16[768,1536]{1,0:T(8,128)(2,1)S(1)}, bf16[768,1536]{1,0:T(8,128)(2,1)}, u32[]{:S(2)}, u32[]{:S(2)}) collective-permute-start(bf16[768,1536]{1,0:T(8,128)(2,1)S(1)} %constant_dynamic-update-slice_fusion.rest_0_), channel_id=1, source_target_pairs={{0,8},{4,12},{8,16},{12,20},{16,24},{20,28},{1,9},{5,13},{9,17},{1... | collective-permute-start | bytes 7077896 | tf_op jit(solution)/shard_map/ppermute | solution.py:255
  15.6 56.4 %collective-permute-start.1 = (bf16[768,1536]{1,0:T(8,128)(2,1)S(1)}, bf16[768,1536]{1,0:T(8,128)(2,1)}, u32[]{:S(2)}, u32[]{:S(2)}) collective-permute-start(bf16[768,1536]{1,0:T(8,128)(2,1)S(1)} %constant_dynamic-update-slice_fusion.rest_0_), channel_id=1, source_target_pairs={{8,0},{12,4},{16,8},{20,12},{24,16},{28,20},{9,1},{13,5},{17,9},{2... | collective-permute-start | bytes 7077896 | tf_op jit(solution)/shard_map/ppermute | solution.py:256
  72.0 55.7 %collective-permute-start.2 = (bf16[768,1536]{1,0:T(8,128)(2,1)}, bf16[768,1536]{1,0:T(8,128)(2,1)}, u32[]{:S(2)}, u32[]{:S(2)}) collective-permute-start(bf16[768,1536]{1,0:T(8,128)(2,1)} %collective-permute-done.rest_2_), channel_id=1, source_target_pairs={{8,16},{12,20},{16,24},{20,28},{9,17},{13,21},{17,25},{21,29},{10,... | collective-permute-start | bytes 7077896 | tf_op jit(solution)/shard_map/ppermute | solution.py:255
  74.2 56.6 %collective-permute-start.3 = (bf16[768,1536]{1,0:T(8,128)(2,1)}, bf16[768,1536]{1,0:T(8,128)(2,1)}, u32[]{:S(2)}, u32[]{:S(2)}) collective-permute-start(bf16[768,1536]{1,0:T(8,128)(2,1)} %collective-permute-done.1.rest_3_), channel_id=1, source_target_pairs={{8,0},{12,4},{16,8},{20,12},{9,1},{13,5},{17,9},{21,13},{10,2},{14... | collective-permute-start | bytes 7077896 | tf_op jit(solution)/shard_map/ppermute | solution.py:256
  92.8 41.5 %copy-start.3 = (bf16[1024,2,256]{2,1,0:T(2,128)(2,1)S(1)}, bf16[1024,2,256]{2,1,0:T(2,128)(2,1)}, u32[]{:S(2)}) copy-start(bf16[1024,2,256]{2,1,0:T(2,128)(2,1)} %param.25) | copy-start | bytes 3145732
  130.8 39.1 %collective-permute-start.4 = (bf16[768,1536]{1,0:T(8,128)(2,1)}, bf16[768,1536]{1,0:T(8,128)(2,1)}, u32[]{:S(2)}, u32[]{:S(2)}) collective-permute-start(bf16[768,1536]{1,0:T(8,128)(2,1)} %collective-permute-done.2.rest_6_), channel_id=1, source_target_pairs={{16,24},{20,28},{17,25},{21,29},{18,26},{22,30},{19,27},{23,31}} | collective-permute-start | bytes 7077896 | tf_op jit(solution)/shard_map/ppermute | solution.py:255
  132.8 82.5 %collective-permute-start.5 = (bf16[768,1536]{1,0:T(8,128)(2,1)}, bf16[768,1536]{1,0:T(8,128)(2,1)}, u32[]{:S(2)}, u32[]{:S(2)}) collective-permute-start(bf16[768,1536]{1,0:T(8,128)(2,1)} %collective-permute-done.3.rest_7_), channel_id=1, source_target_pairs={{8,0},{12,4},{9,1},{13,5},{10,2},{14,6},{11,3},{15,7}} | collective-permute-start | bytes 7077896 | tf_op jit(solution)/shard_map/ppermute | solution.py:256
  159.7 164.0 %copy-start.5 = (bf16[3,2,1536]{2,1,0:T(2,128)(2,1)S(1)}, bf16[3,2,1536]{2,1,0:T(2,128)(2,1)}, u32[]{:S(2)}) copy-start(bf16[3,2,1536]{2,1,0:T(2,128)(2,1)} %param.36) | copy-start | bytes 55300
  215.4 54.2 %collective-permute-start.7 = (bf16[768,1536]{1,0:T(8,128)(2,1)S(1)}, bf16[768,1536]{1,0:T(8,128)(2,1)S(1)}, u32[]{:S(2)}, u32[]{:S(2)}) collective-permute-start(bf16[768,1536]{1,0:T(8,128)(2,1)S(1)} %constant_dynamic-update-slice_fusion.rest_0_), channel_id=1, source_target_pairs={{0,4},{4,0},{8,12},{12,8},{16,20},{20,16},{24,28},{28,24},{1,5},{5... | collective-permute-start | bytes 7077896 | tf_op jit(solution)/shard_map/ppermute | solution.py:239
  217.0 56.1 %collective-permute-start.8 = (bf16[768,1536]{1,0:T(8,128)(2,1)}, bf16[768,1536]{1,0:T(8,128)(2,1)}, u32[]{:S(2)}, u32[]{:S(2)}) collective-permute-start(bf16[768,1536]{1,0:T(8,128)(2,1)} %collective-permute-done.rest_2_), channel_id=1, source_target_pairs={{8,12},{12,8},{16,20},{20,16},{24,28},{28,24},{9,13},{13,9},{17,21... | collective-permute-start | bytes 7077896 | tf_op jit(solution)/shard_map/ppermute | solution.py:239
  219.1 101.1 %collective-permute-start.9 = (bf16[768,1536]{1,0:T(8,128)(2,1)}, bf16[768,1536]{1,0:T(8,128)(2,1)}, u32[]{:S(2)}, u32[]{:S(2)}) collective-permute-start(bf16[768,1536]{1,0:T(8,128)(2,1)} %collective-permute-done.1.rest_3_), channel_id=1, source_target_pairs={{0,4},{4,0},{8,12},{12,8},{16,20},{20,16},{1,5},{5,1},{9,13},{13,9... | collective-permute-start | bytes 7077896 | tf_op jit(solution)/shard_map/ppermute | solution.py:239
  221.5 102.2 %collective-permute-start.10 = (bf16[768,1536]{1,0:T(8,128)(2,1)}, bf16[768,1536]{1,0:T(8,128)(2,1)}, u32[]{:S(2)}, u32[]{:S(2)}) collective-permute-start(bf16[768,1536]{1,0:T(8,128)(2,1)} %collective-permute-done.2.rest_6_), channel_id=1, source_target_pairs={{16,20},{20,16},{24,28},{28,24},{17,21},{21,17},{25,29},{29,25},{1... | collective-permute-start | bytes 7077896 | tf_op jit(solution)/shard_map/ppermute | solution.py:239
  223.7 147.2 %collective-permute-start.11 = (bf16[768,1536]{1,0:T(8,128)(2,1)}, bf16[768,1536]{1,0:T(8,128)(2,1)}, u32[]{:S(2)}, u32[]{:S(2)}) collective-permute-start(bf16[768,1536]{1,0:T(8,128)(2,1)} %collective-permute-done.3.rest_7_), channel_id=1, source_target_pairs={{0,4},{4,0},{8,12},{12,8},{1,5},{5,1},{9,13},{13,9},{2,6},{6,2},{1... | collective-permute-start | bytes 7077896 | tf_op jit(solution)/shard_map/ppermute | solution.py:239
  269.6 1.4 copy-start
  271.0 99.8 %collective-permute-start.12 = (bf16[768,1536]{1,0:T(8,128)(2,1)}, bf16[768,1536]{1,0:T(8,128)(2,1)}, u32[]{:S(2)}, u32[]{:S(2)}) collective-permute-start(bf16[768,1536]{1,0:T(8,128)(2,1)} %collective-permute-done.4.rest_10_), channel_id=1, source_target_pairs={{24,28},{28,24},{25,29},{29,25},{26,30},{30,26},{27,31},{31,27}} | collective-permute-start | bytes 7077896 | tf_op jit(solution)/shard_map/ppermute | solution.py:239
  273.1 145.2 %collective-permute-start.13 = (bf16[768,1536]{1,0:T(8,128)(2,1)}, bf16[768,1536]{1,0:T(8,128)(2,1)}, u32[]{:S(2)}, u32[]{:S(2)}) collective-permute-start(bf16[768,1536]{1,0:T(8,128)(2,1)} %collective-permute-done.5.rest_11_), channel_id=1, source_target_pairs={{0,4},{4,0},{1,5},{5,1},{2,6},{6,2},{3,7},{7,3}} | collective-permute-start | bytes 7077896 | tf_op jit(solution)/shard_map/ppermute | solution.py:239
  320.3 98.3 %collective-permute-start.6 = (bf16[16,2048]{1,0:T(8,128)(2,1)S(1)}, bf16[16,2048]{1,0:T(8,128)(2,1)S(1)}, u32[]{:S(2)}, u32[]{:S(2)}) collective-permute-start(bf16[16,2048]{1,0:T(8,128)(2,1)S(1)} %slice.4), channel_id=1, source_target_pairs={{0,4},{4,8},{8,12},{12,16},{16,20},{20,24},{24,28},{1,5},{5,9},{9,... | collective-permute-start | bytes 196616 | tf_op jit(solution)/shard_map/ppermute | solution.py:24
  460.9 31.8 %copy-start.1 = (f32[256,2048]{1,0:T(8,128)S(1)}, f32[256,2048]{1,0:T(8,128)}, u32[]{:S(2)}) copy-start(f32[256,2048]{1,0:T(8,128)} %get-tuple-element.44) | copy-start | bytes 6291460
  460.9 4.5 collective-permute-start.14
  467.3 25.4 %collective-permute-start.15 = (bf16[256,2048]{1,0:T(8,128)(2,1)S(1)}, bf16[256,2048]{1,0:T(8,128)(2,1)}, u32[]{:S(2)}, u32[]{:S(2)}) collective-permute-start(bf16[256,2048]{1,0:T(8,128)(2,1)S(1)} %fusion), channel_id=1, source_target_pairs={{0,2},{1,3},{2,0},{3,1},{4,6},{5,7},{6,4},{7,5},{8,10},{9,11},{10,... | collective-permute-start | bytes 3145736 | tf_op jit(solution)/shard_map/ppermute | solution.py:617
Sparse Core Ops, SparseCore 0:
  215.5 35.1 all-gather.1

commit v2 on v1

--- a/solution.py
+++ b/solution.py
@@ -426,7 +426,7 @@
 
     @pl.when(pl.program_id(0) == 0)
     def _():
-        copies = load_pieces(meta, refs, ((2 * rows, 3 * rows),), (down_w,), sem)
+        copies = load_pieces(meta, refs, ((0, rows),), (down_w,), sem)
         finish_pieces(copies)
 
     wide = out_ref.shape[1]
@@ -540,9 +540,7 @@
     gates_beta = jnp.concatenate([level, beta_rate], axis=0).reshape(-1, length)
     gates_beta = jnp.pad(gates_beta, ((0, -gates_beta.shape[0] % 8), (0, 0)))
     spare = -latter_request_vectors.shape[1] % LANES
-    sides = jnp.concatenate(
-        [switching_channel_map, broadening_channel_map, narrowing_map_weights_in], axis=0
-    )
+    sides = jnp.concatenate([switching_channel_map, broadening_channel_map], axis=0)
     side = line_step(line_start(sides), 1)
     units = former_request_vectors.shape[1] // LANES + (
         latter_request_vectors.shape[1] + spare
@@ -560,14 +558,15 @@
     done = ()
     summary = None
     for part in range(parts):
-        if part == parts - 1:
+        if part == parts // 2:
             side, running = tie(side, running)
             side = line_step(line_swap(side, 1), 2)
         *done, running, summary = local_terms(*drawn, running, part, parts, tuple(done))
     g_part, h_part = done
     everyone = exchange(summary)
-    side, everyone = tie(side, everyone)
+    side, (everyone, narrow) = tie(side, (everyone, narrowing_map_weights_in))
     side = line_step(line_swap(side, 2), 3)
+    down = line_step(line_start(narrow), 1)
     place = lax.axis_index("sp").astype(jnp.int32).reshape(1)
     attended = finish_heads(
         place,
@@ -590,11 +589,15 @@
     side, normed = tie(side, normed)
     side = line_rest(line_swap(side, 3), 4)
     features = lax.all_gather(normed, "tp", axis=0, tiled=True)
+    down = line_step(line_swap(down, 1), 2)
     edge = 16
     halo = from_behind(features[-edge:], "sp", 1)
     taps = timewise_convolve_tapvalues.astype(F32).reshape(2 * TAPS, -1)
+    down, halo = tie(down, halo)
+    down = line_step(line_swap(down, 2), 3)
     hidden = up_part(features, halo, taps, side["pieces"])
-    partial = down_part(hidden, features.shape[1], side["pieces"])
+    down = line_rest(line_swap(down, 3), 4)
+    partial = down_part(hidden, features.shape[1], down["pieces"])
     return (skip_stream + team_sum(partial)).astype(jnp.bfloat16)
 
 

time: 504 us -> 449 us (0.89); the launches traced: 503 us -> 441 us
  waiting for transfers between devices: 257 us -> 171 us
  starting transfers between devices: 36.8 us -> 58.1 us
    ppermute x7 -> x14, waiting for transfers between devices: 180 us -> 65.9 us  [swapped(): return lax.ppermute(value, 'sp', [(i, i ^ 1) for i in places])]
    ppermute x1, waiting for transfers between devices: 0.34 us -> 19.4 us  [from_behind(): lax.ppermute(value, axis, [(source, source + steps) for source in range(l...]
    ppermute x3 -> x6, starting transfers between devices: 10.6 us -> 20.2 us  [line_step(): right = lax.ppermute(line['right'], 'sp', up)]
    ppermute x3 -> x6, waiting for transfers between devices: 48.5 us -> 57.5 us  [line_step(): left = lax.ppermute(line['left'], 'sp', down)]
    ppermute x7 -> x14, starting transfers between devices: 17.1 us -> 25.5 us  [swapped(): return lax.ppermute(value, 'sp', [(i, i ^ 1) for i in places])]
  transfers between devices with their start and end apart: 17 -> 30, of which waited for: 9 -> 9; matrix products, arithmetic and copies ran while one was open for 1% -> 1% of each run, Pallas kernels for 24% -> 33%
where the time goes in v2:
time: 449 us; the launch traced here: 441 us
  waiting for transfers between devices  171 us (38%)
  Pallas kernels  159 us (35%)
  starting transfers between devices  58.1 us (13%)
  blocking collectives  18.7 us (4%)
  local copies, waits for them, and re-layouts  14.5 us (3%)
  between operations  14 us (3%)
  other arithmetic  5.89 us (1%)
    pallas_call x4, Pallas kernels, local_terms(): pl.pallas_call(local_kernel, grid=(steps,), in_specs=[pl.BlockSpec((CHUNK...  69.4 us
    ppermute x14, waiting for transfers between devices, swapped(): return lax.ppermute(value, 'sp', [(i, i ^ 1) for i in places])  65.9 us
    ppermute x6, waiting for transfers between devices, line_step(): left = lax.ppermute(line['left'], 'sp', down)  57.5 us
    pallas_call x1, Pallas kernels, exchange(): pl.pallas_call(exchange_kernel, in_specs=[pl.BlockSpec(memory_space=pltpu...  35 us
    pallas_call x1, Pallas kernels, up_part(): pl.pallas_call(functools.partial(up_kernel, meta), grid=(length // tile,)...  26.2 us
    ppermute x14, starting transfers between devices, swapped(): return lax.ppermute(value, 'sp', [(i, i ^ 1) for i in places])  25.5 us
    ppermute x1, waiting for transfers between devices, team_sum(): lax.ppermute(both(1 - place).astype(BF16), 'tp', [(i, i ^ 2) for i in ran...  24 us
    ppermute x6, starting transfers between devices, line_step(): right = lax.ppermute(line['right'], 'sp', up)  20.2 us
  transfers between devices with their start and end apart: 30, of which 9 were waited for; matrix products, arithmetic and copies ran while one was open for 1% of the time, Pallas kernels for 33%

profile of v2, /device:TPU:0, one launch (start us, length us, event | category | flops | bytes accessed | tf_op | source)
XLA Modules:
  0.0 441.0 jit_solution(13455531445834477125)
XLA Ops:
  6.5 1.3 constant_dynamic-update-slice_fusion.1
  8.0 6.1 %collective-permute-start = (bf16[512,1536]{1,0:T(8,128)(2,1)S(1)}, bf16[512,1536]{1,0:T(8,128)(2,1)}, u32[]{:S(2)}, u32[]{:S(2)}) collective-permute-start(bf16[512,1536]{1,0:T(8,128)(2,1)S(1)} %constant_dynamic-update-slice_fusion.rest_0_), channel_id=1, source_target_pairs={{0,8},{4,12},{8,16},{12,20},{16,24},{20,28},{1,9},{5,13},{9,17},{1... | collective-permute-start | bytes 4718600 | tf_op jit(solution)/shard_map/ppermute | solution.py:255
  14.1 1.3 collective-permute-start.1
  15.4 1.2 copy.26
  18.3 17.4 %shard_map.181 = (bf16[1024,512]{1,0:T(8,128)(2,1)}, f32[1024,512]{1,0:T(8,128)}, f32[3,128,256]{2,1,0:T(8,128)}, bf16[3,128,256]{2,1,0:T(8,128)(2,1)}) custom-call(bf16[1024,256]{1,0:T(8,128)(2,1)} %q1_ref.7, bf16[1024,256]{1,0:T(8,128)(2,1)} %k1_ref.7, bf16[1024,128]{1,0:T(8,128)(2,1)} %q2_ref.7, bf16[1024,128]{1,0:T(8,128)(2,1)} %k2_ref.7, ...), custom_call_target="tpu_custom_call" | custom-call | flops 6710886400 | bytes 5242880 | tf_op jit(solution)/shard_map/pallas_call | solution.py:152
  35.7 17.3 %shard_map.182 = (bf16[1024,512]{1,0:T(8,128)(2,1)}, f32[1024,512]{1,0:T(8,128)}, f32[3,128,256]{2,1,0:T(8,128)}, bf16[3,128,256]{2,1,0:T(8,128)(2,1)}) custom-call(bf16[1024,256]{1,0:T(8,128)(2,1)} %q1_ref.7, bf16[1024,256]{1,0:T(8,128)(2,1)} %k1_ref.7, bf16[1024,128]{1,0:T(8,128)(2,1)} %q2_ref.7, ...), custom_call_target="tpu_custom_call", output_to_operand_aliasing={{0}: (7, {}), {1}: (8, {})} | custom-call | flops 6710886400 | bytes 5242880 | tf_op jit(solution)/shard_map/pallas_call | solution.py:152
  53.0 1.8 collective-permute-start.2
  54.8 1.3 collective-permute-start.3
  56.1 17.4 %shard_map.183 = (bf16[1024,512]{1,0:T(8,128)(2,1)}, f32[1024,512]{1,0:T(8,128)}, f32[3,128,256]{2,1,0:T(8,128)}, bf16[3,128,256]{2,1,0:T(8,128)(2,1)}) custom-call(bf16[1024,256]{1,0:T(8,128)(2,1)} %q1_ref.7, bf16[1024,256]{1,0:T(8,128)(2,1)} %k1_ref.7, bf16[1024,128]{1,0:T(8,128)(2,1)} %q2_ref.7, ...), custom_call_target="tpu_custom_call", output_to_operand_aliasing={{0}: (7, {}), {1}: (8, {})} | custom-call | flops 6710886400 | bytes 5242880 | tf_op jit(solution)/shard_map/pallas_call | solution.py:152
  73.5 17.4 %shard_map.184 = (bf16[1024,512]{1,0:T(8,128)(2,1)}, f32[1024,512]{1,0:T(8,128)}, f32[3,128,256]{2,1,0:T(8,128)}, bf16[3,128,256]{2,1,0:T(8,128)(2,1)}) custom-call(bf16[1024,256]{1,0:T(8,128)(2,1)} %q1_ref.7, bf16[1024,256]{1,0:T(8,128)(2,1)} %k1_ref.7, bf16[1024,128]{1,0:T(8,128)(2,1)} %q2_ref.7, ...), custom_call_target="tpu_custom_call", output_to_operand_aliasing={{0}: (7, {}), {1}: (8, {})} | custom-call | flops 6710886400 | bytes 5242880 | tf_op jit(solution)/shard_map/pallas_call | solution.py:152
  90.9 35.0 %shard_map.185.all_ref = bf16[8,3,128,256]{3,2,1,0:T(8,128)(2,1)} custom-call(bf16[3,128,256]{2,1,0:T(8,128)(2,1)} %get-tuple-element.42.own_ref), custom_call_target="tpu_custom_call" | custom-call | flops 1000000000 | bytes 1000000 | tf_op jit(solution)/shard_map/pallas_call | solution.py:226
  125.9 1.8 collective-permute-start.4
  127.7 1.5 collective-permute-start.5
  129.2 1.2 copy.27
  130.4 5.5 %shard_map.186 = bf16[1024,512]{1,0:T(8,128)(2,1)} custom-call(s32[1]{0:T(128)} %bitcast.place_ref, bf16[8,3,128,256]{3,2,1,0:T(8,128)(2,1)} %shard_map.185.all_ref, bf16[1024,512]{1,0:T(8,128)(2,1)} %get-tuple-element.46.g_ref, f32[1024,512]{1,0:T(8,128)} %get-tuple-element.47.h_ref, bf16[1024,512]{1,0:T(8,128)(2,1)} %bitcast.26, f32[1,128]{1,0:T(1,128)} %bitcast.35), custom_call_target="tpu_custom_call" | custom-call | flops 1073741824 | bytes 5242880 | tf_op jit(solution)/shard_map/pallas_call | solution.py:490
  135.9 18.7 %all_to_all.5.x_ref = bf16[4,256,512]{2,1,0:T(8,128)(2,1)} all-to-all(bf16[4,256,512]{2,1,0:T(8,128)(2,1)} %bitcast.27), channel_id=1, replica_groups=mesh['sp'=8,'tp'=4] {'tp'}, dimensions={0} | all-to-all | bytes 2097152 | tf_op jit(solution)/shard_map/all_to_all | solution.py:580
  154.6 10.1 %shard_map.187 = (f32[256,2048]{1,0:T(8,128)}, bf16[256,2048]{1,0:T(8,128)(2,1)}) custom-call(bf16[4,256,512]{2,1,0:T(8,128)(2,1)} %all_to_all.5.x_ref, bf16[2048,2048]{1,0:T(8,128)(2,1)} %w_ref.1, bf16[256,2048]{1,0:T(8,128)(2,1)} %skip_ref.1, f32[1,2048]{1,0:T(1,128)} %bitcast.34), custom_call_target="tpu_custom_call" | custom-call | flops 2147483648 | bytes 8388608 | tf_op jit(solution)/shard_map/pallas_call | solution.py:337
  164.8 5.9 %collective-permute-done.5.rest_11_ = bf16[512,1536]{1,0:T(8,128)(2,1)} collective-permute-done((bf16[512,1536]{1,0:T(8,128)(2,1)}, bf16[512,1536]{1,0:T(8,128)(2,1)}, u32[]{:S(2)}, u32[]{:S(2)}) %collective-permute-start.5) | collective-permute-done | bytes 1572896 | tf_op jit(solution)/shard_map/ppermute | solution.py:256
  172.1 3.4 collective-permute-start.13
  175.5 8.2 %collective-permute-start.7 = (bf16[256,1536]{1,0:T(8,128)(2,1)}, bf16[256,1536]{1,0:T(8,128)(2,1)S(1)}, u32[]{:S(2)}, u32[]{:S(2)}) collective-permute-start(bf16[256,1536]{1,0:T(8,128)(2,1)} %rest_0_), channel_id=1, source_target_pairs={{0,8},{4,12},{8,16},{12,20},{16,24},{20,28},{1,9},{5,13},{9,17},{1... | collective-permute-start | bytes 2359304 | tf_op jit(solution)/shard_map/ppermute | solution.py:255
  183.6 1.3 collective-permute-start.9
  184.9 23.1 %collective-permute-done.11.rest_1_ = bf16[512,1536]{1,0:T(8,128)(2,1)S(1)} collective-permute-done((bf16[512,1536]{1,0:T(8,128)(2,1)S(1)}, bf16[512,1536]{1,0:T(8,128)(2,1)S(1)}, u32[]{:S(2)}, u32[]{:S(2)}) %collective-permute-start.11) | collective-permute-done | bytes 1572896 | tf_op jit(solution)/shard_map/ppermute | solution.py:239
  210.2 1.8 collective-permute-start.14
  212.0 29.7 %collective-permute-done.13.rest_5_ = bf16[512,1536]{1,0:T(8,128)(2,1)S(1)} collective-permute-done((bf16[512,1536]{1,0:T(8,128)(2,1)}, bf16[512,1536]{1,0:T(8,128)(2,1)S(1)}, u32[]{:S(2)}, u32[]{:S(2)}) %collective-permute-start.13) | collective-permute-done | bytes 1572896 | tf_op jit(solution)/shard_map/ppermute | solution.py:239
  241.7 2.5 collective-permute-start.15
  244.2 1.3 collective-permute-start.10
  245.5 13.1 %collective-permute-done.18.rest_1_ = bf16[256,1536]{1,0:T(8,128)(2,1)S(1)} collective-permute-done((bf16[256,1536]{1,0:T(8,128)(2,1)}, bf16[256,1536]{1,0:T(8,128)(2,1)S(1)}, u32[]{:S(2)}, u32[]{:S(2)}) %collective-permute-start.18) | collective-permute-done | bytes 786464 | tf_op jit(solution)/shard_map/ppermute | solution.py:239
  259.5 1.8 collective-permute-start.16
  262.2 2.5 collective-permute-start.17
  265.5 33.6 %collective-permute-done.10.rest_7_ = bf16[256,1536]{1,0:T(8,128)(2,1)} collective-permute-done((bf16[256,1536]{1,0:T(8,128)(2,1)}, bf16[256,1536]{1,0:T(8,128)(2,1)}, u32[]{:S(2)}, u32[]{:S(2)}) %collective-permute-start.10) | collective-permute-done | bytes 786464 | tf_op jit(solution)/shard_map/ppermute | solution.py:256
  299.2 3.2 collective-permute-start.6
  302.4 19.4 %collective-permute-done.6.halo_ref = bf16[16,2048]{1,0:T(8,128)(2,1)S(1)} collective-permute-done((bf16[16,2048]{1,0:T(8,128)(2,1)S(1)}, bf16[16,2048]{1,0:T(8,128)(2,1)S(1)}, u32[]{:S(2)}, u32[]{:S(2)}) %collective-permute-start.6) | collective-permute-done | bytes 65568 | tf_op jit(solution)/shard_map/ppermute | solution.py:24
  321.8 1.6 collective-permute-start.19
  323.4 1.6 collective-permute-start.23
  324.9 1.3 collective-permute-start.24
  326.3 4.5 %collective-permute-start.20 = (bf16[256,1536]{1,0:T(8,128)(2,1)}, bf16[256,1536]{1,0:T(8,128)(2,1)S(1)}, u32[]{:S(2)}, u32[]{:S(2)}) collective-permute-start(bf16[256,1536]{1,0:T(8,128)(2,1)} %collective-permute-done.9.rest_3_), channel_id=1, source_target_pairs={{0,4},{4,0},{8,12},{12,8},{16,20},{20,16},{1,5},{5,1},{9,13},{13,9... | collective-permute-start | bytes 2359304 | tf_op jit(solution)/shard_map/ppermute | solution.py:239
  331.6 1.9 collective-permute-start.22
  334.3 18.0 %collective-permute-done.24.rest_11_ = bf16[256,1536]{1,0:T(8,128)(2,1)} collective-permute-done((bf16[256,1536]{1,0:T(8,128)(2,1)}, bf16[256,1536]{1,0:T(8,128)(2,1)}, u32[]{:S(2)}, u32[]{:S(2)}) %collective-permute-start.24) | collective-permute-done | bytes 786464 | tf_op jit(solution)/shard_map/ppermute | solution.py:256
  352.2 2.2 collective-permute-start.26
  354.4 26.2 %shard_map.188.x_ref = bf16[1024,1536]{1,0:T(8,128)(2,1)} custom-call(bf16[1024,2048]{1,0:T(8,128)(2,1)} %all-gather.2.cloned.1.call-done.x_ref, bf16[16,2048]{1,0:T(8,128)(2,1)S(1)} %collective-permute-done.6.halo_ref, f32[6,1536]{1,0:T(8,128)S(1)} %reshape.55.taps_ref, bf16[512,1536]{1,0:T(8,128)(2,1)S(1)} %constant_dynamic-update-slice_fusion.rest_0_, ...), custom_call_target="tpu_custom_call" | custom-call | flops 12884901888 | bytes 12582912 | tf_op jit(solution)/shard_map/pallas_call | solution.py:399
  382.3 0.9 copy-done.21
  383.2 12.3 %shard_map.189 = bf16[1024,2048]{1,0:T(8,128)(2,1)} custom-call(bf16[1024,1536]{1,0:T(8,128)(2,1)} %shard_map.188.x_ref, bf16[256,1536]{1,0:T(8,128)(2,1)S(1)} %copy-done, bf16[256,1536]{1,0:T(8,128)(2,1)S(1)} %copy-done.4, bf16[256,1536]{1,0:T(8,128)(2,1)S(1)} %copy-done.2, bf16[256,1536]{1,0:T(8,128)(2,1)} %collective-permute-done.9.rest_3_, ...), custom_call_target="tpu_custom_call" | custom-call | flops 6442450944 | bytes 6291456 | tf_op jit(solution)/shard_map/pallas_call | solution.py:443
  395.6 3.1 dynamic-slice_bitcast_fusion
  398.7 4.5 %collective-permute-done.27 = bf16[2,256,2048]{2,1,0:T(8,128)(2,1)} collective-permute-done((bf16[2,256,2048]{2,1,0:T(8,128)(2,1)}, bf16[2,256,2048]{2,1,0:T(8,128)(2,1)}, u32[]{:S(2)}, u32[]{:S(2)}) %collective-permute-start.27) | collective-permute-done | bytes 2097184 | tf_op jit(solution)/shard_map/ppermute | solution.py:612
  403.2 1.9 fusion
  405.2 1.3 collective-permute-start.28
  406.5 24.0 %collective-permute-done.28 = bf16[256,2048]{1,0:T(8,128)(2,1)S(1)} collective-permute-done((bf16[256,2048]{1,0:T(8,128)(2,1)S(1)}, bf16[256,2048]{1,0:T(8,128)(2,1)S(1)}, u32[]{:S(2)}, u32[]{:S(2)}) %collective-permute-start.28) | collective-permute-done | bytes 1048608 | tf_op jit(solution)/shard_map/ppermute | solution.py:620
  430.4 3.7 fusion.3
  (83 shorter events, 11.1 us)
Async XLA Ops:
  6.5 1.4 copy-start.7
  6.5 8.9 %copy-start.5 = (bf16[1024,2,256]{2,1,0:T(2,128)(2,1)S(1)}, bf16[1024,2,256]{2,1,0:T(2,128)(2,1)}, u32[]{:S(2)}) copy-start(bf16[1024,2,256]{2,1,0:T(2,128)(2,1)} %param.24) | copy-start | bytes 3145732
  6.5 258.2 %all-gather.2.cloned.1.call-start = ((), (), s32[]{:S(2)}) async-start(), calls=%async_computation.1 | async-start | bytes 5242880 | tf_op jit(solution)/shard_map/all_gather | solution.py:591
  7.9 8.7 %copy-start.13 = (f32[2,2]{1,0:T(2,128)S(1)}, f32[2,2]{1,0:T(2,128)}, u32[]{:S(2)}) copy-start(f32[2,2]{1,0:T(2,128)} %param.29) | copy-start | bytes 52
  7.9 8.7 %copy-start.9 = (f32[2,2,1024]{2,1,0:T(2,128)S(1)}, f32[2,2,1024]{2,1,0:T(2,128)}, u32[]{:S(2)}) copy-start(f32[2,2,1024]{2,1,0:T(2,128)} %param.28) | copy-start | bytes 49156
  7.9 8.7 %copy-start.10 = (f32[2,2,1024]{2,1,0:T(2,128)S(1)}, f32[2,2,1024]{2,1,0:T(2,128)}, u32[]{:S(2)}) copy-start(f32[2,2,1024]{2,1,0:T(2,128)} %param.27) | copy-start | bytes 49156
  7.9 8.7 %copy-start.11 = (bf16[2,2,1024]{2,1,0:T(2,128)(2,1)S(1)}, bf16[2,2,1024]{2,1,0:T(2,128)(2,1)}, u32[]{:S(2)}) copy-start(bf16[2,2,1024]{2,1,0:T(2,128)(2,1)} %param.26) | copy-start | bytes 24580
  7.9 8.7 %copy-start.12 = (f32[2,2]{1,0:T(2,128)S(1)}, f32[2,2]{1,0:T(2,128)}, u32[]{:S(2)}) copy-start(f32[2,2]{1,0:T(2,128)} %param.30) | copy-start | bytes 52
  8.0 45.0 %collective-permute-start = (bf16[512,1536]{1,0:T(8,128)(2,1)S(1)}, bf16[512,1536]{1,0:T(8,128)(2,1)}, u32[]{:S(2)}, u32[]{:S(2)}) collective-permute-start(bf16[512,1536]{1,0:T(8,128)(2,1)S(1)} %constant_dynamic-update-slice_fusion.rest_0_), channel_id=1, source_target_pairs={{0,8},{4,12},{8,16},{12,20},{16,24},{20,28},{1,9},{5,13},{9,17},{1... | collective-permute-start | bytes 4718600 | tf_op jit(solution)/shard_map/ppermute | solution.py:255
  14.1 38.9 %collective-permute-start.1 = (bf16[512,1536]{1,0:T(8,128)(2,1)S(1)}, bf16[512,1536]{1,0:T(8,128)(2,1)}, u32[]{:S(2)}, u32[]{:S(2)}) collective-permute-start(bf16[512,1536]{1,0:T(8,128)(2,1)S(1)} %constant_dynamic-update-slice_fusion.rest_0_), channel_id=1, source_target_pairs={{8,0},{12,4},{16,8},{20,12},{24,16},{28,20},{9,1},{13,5},{17,9},{2... | collective-permute-start | bytes 4718600 | tf_op jit(solution)/shard_map/ppermute | solution.py:256
  53.0 72.8 %collective-permute-start.2 = (bf16[512,1536]{1,0:T(8,128)(2,1)}, bf16[512,1536]{1,0:T(8,128)(2,1)}, u32[]{:S(2)}, u32[]{:S(2)}) collective-permute-start(bf16[512,1536]{1,0:T(8,128)(2,1)} %collective-permute-done.rest_2_), channel_id=1, source_target_pairs={{8,16},{12,20},{16,24},{20,28},{9,17},{13,21},{17,25},{21,29},{10,... | collective-permute-start | bytes 4718600 | tf_op jit(solution)/shard_map/ppermute | solution.py:255
  54.8 71.0 %collective-permute-start.3 = (bf16[512,1536]{1,0:T(8,128)(2,1)}, bf16[512,1536]{1,0:T(8,128)(2,1)}, u32[]{:S(2)}, u32[]{:S(2)}) collective-permute-start(bf16[512,1536]{1,0:T(8,128)(2,1)} %collective-permute-done.1.rest_3_), channel_id=1, source_target_pairs={{8,0},{12,4},{16,8},{20,12},{9,1},{13,5},{17,9},{21,13},{10,2},{14... | collective-permute-start | bytes 4718600 | tf_op jit(solution)/shard_map/ppermute | solution.py:256
  90.9 38.3 %copy-start.6 = (bf16[1024,2,256]{2,1,0:T(2,128)(2,1)S(1)}, bf16[1024,2,256]{2,1,0:T(2,128)(2,1)}, u32[]{:S(2)}) copy-start(bf16[1024,2,256]{2,1,0:T(2,128)(2,1)} %param.25) | copy-start | bytes 3145732
  125.9 38.9 %collective-permute-start.4 = (bf16[512,1536]{1,0:T(8,128)(2,1)}, bf16[512,1536]{1,0:T(8,128)(2,1)}, u32[]{:S(2)}, u32[]{:S(2)}) collective-permute-start(bf16[512,1536]{1,0:T(8,128)(2,1)} %collective-permute-done.2.rest_6_), channel_id=1, source_target_pairs={{16,24},{20,28},{17,25},{21,29},{18,26},{22,30},{19,27},{23,31}} | collective-permute-start | bytes 4718600 | tf_op jit(solution)/shard_map/ppermute | solution.py:255
  127.7 42.9 %collective-permute-start.5 = (bf16[512,1536]{1,0:T(8,128)(2,1)}, bf16[512,1536]{1,0:T(8,128)(2,1)}, u32[]{:S(2)}, u32[]{:S(2)}) collective-permute-start(bf16[512,1536]{1,0:T(8,128)(2,1)} %collective-permute-done.3.rest_7_), channel_id=1, source_target_pairs={{8,0},{12,4},{9,1},{13,5},{10,2},{14,6},{11,3},{15,7}} | collective-permute-start | bytes 4718600 | tf_op jit(solution)/shard_map/ppermute | solution.py:256
  154.6 171.6 %copy-start.8 = (bf16[3,2,1536]{2,1,0:T(2,128)(2,1)S(1)}, bf16[3,2,1536]{2,1,0:T(2,128)(2,1)}, u32[]{:S(2)}) copy-start(bf16[3,2,1536]{2,1,0:T(2,128)(2,1)} %param.36) | copy-start | bytes 55300
  170.7 37.3 %collective-permute-start.11 = (bf16[512,1536]{1,0:T(8,128)(2,1)S(1)}, bf16[512,1536]{1,0:T(8,128)(2,1)S(1)}, u32[]{:S(2)}, u32[]{:S(2)}) collective-permute-start(bf16[512,1536]{1,0:T(8,128)(2,1)S(1)} %constant_dynamic-update-slice_fusion.rest_0_), channel_id=1, source_target_pairs={{0,4},{4,0},{8,12},{12,8},{16,20},{20,16},{24,28},{28,24},{1,5},{5... | collective-permute-start | bytes 4718600 | tf_op jit(solution)/shard_map/ppermute | solution.py:239
  171.3 38.9 %collective-permute-start.12 = (bf16[512,1536]{1,0:T(8,128)(2,1)}, bf16[512,1536]{1,0:T(8,128)(2,1)S(1)}, u32[]{:S(2)}, u32[]{:S(2)}) collective-permute-start(bf16[512,1536]{1,0:T(8,128)(2,1)} %collective-permute-done.rest_2_), channel_id=1, source_target_pairs={{8,12},{12,8},{16,20},{20,16},{24,28},{28,24},{9,13},{13,9},{17,21... | collective-permute-start | bytes 4718600 | tf_op jit(solution)/shard_map/ppermute | solution.py:239
  172.1 69.6 %collective-permute-start.13 = (bf16[512,1536]{1,0:T(8,128)(2,1)}, bf16[512,1536]{1,0:T(8,128)(2,1)S(1)}, u32[]{:S(2)}, u32[]{:S(2)}) collective-permute-start(bf16[512,1536]{1,0:T(8,128)(2,1)} %collective-permute-done.1.rest_3_), channel_id=1, source_target_pairs={{0,4},{4,0},{8,12},{12,8},{16,20},{20,16},{1,5},{5,1},{9,13},{13,9... | collective-permute-start | bytes 4718600 | tf_op jit(solution)/shard_map/ppermute | solution.py:239
  175.5 33.1 %collective-permute-start.7 = (bf16[256,1536]{1,0:T(8,128)(2,1)}, bf16[256,1536]{1,0:T(8,128)(2,1)S(1)}, u32[]{:S(2)}, u32[]{:S(2)}) collective-permute-start(bf16[256,1536]{1,0:T(8,128)(2,1)} %rest_0_), channel_id=1, source_target_pairs={{0,8},{4,12},{8,16},{12,20},{16,24},{20,28},{1,9},{5,13},{9,17},{1... | collective-permute-start | bytes 2359304 | tf_op jit(solution)/shard_map/ppermute | solution.py:255
  183.6 60.6 %collective-permute-start.9 = (bf16[256,1536]{1,0:T(8,128)(2,1)}, bf16[256,1536]{1,0:T(8,128)(2,1)}, u32[]{:S(2)}, u32[]{:S(2)}) collective-permute-start(bf16[256,1536]{1,0:T(8,128)(2,1)} %rest_0_), channel_id=1, source_target_pairs={{8,0},{12,4},{16,8},{20,12},{24,16},{28,20},{9,1},{13,5},{17,9},{2... | collective-permute-start | bytes 2359304 | tf_op jit(solution)/shard_map/ppermute | solution.py:256
  208.0 50.6 %collective-permute-start.18 = (bf16[256,1536]{1,0:T(8,128)(2,1)}, bf16[256,1536]{1,0:T(8,128)(2,1)S(1)}, u32[]{:S(2)}, u32[]{:S(2)}) collective-permute-start(bf16[256,1536]{1,0:T(8,128)(2,1)} %rest_0_), channel_id=1, source_target_pairs={{0,4},{4,0},{8,12},{12,8},{16,20},{20,16},{24,28},{28,24},{1,5},{5... | collective-permute-start | bytes 2359304 | tf_op jit(solution)/shard_map/ppermute | solution.py:239
  209.5 51.8 %collective-permute-start.8 = (bf16[256,1536]{1,0:T(8,128)(2,1)S(1)}, bf16[256,1536]{1,0:T(8,128)(2,1)S(1)}, u32[]{:S(2)}, u32[]{:S(2)}) collective-permute-start(bf16[256,1536]{1,0:T(8,128)(2,1)S(1)} %collective-permute-done.7.rest_2_), channel_id=1, source_target_pairs={{8,16},{12,20},{16,24},{20,28},{9,17},{13,21},{17,25},{21,29},{10,... | collective-permute-start | bytes 2359304 | tf_op jit(solution)/shard_map/ppermute | solution.py:255
  210.2 51.1 %copy-start.14 = (bf16[512,1536]{1,0:T(8,128)(2,1)}, bf16[512,1536]{1,0:T(8,128)(2,1)S(1)}, u32[]{:S(2)}) copy-start(bf16[512,1536]{1,0:T(8,128)(2,1)S(1)} %collective-permute-done.12.rest_4_) | copy-start | bytes 4718596
  210.2 113.1 %collective-permute-start.14 = (bf16[512,1536]{1,0:T(8,128)(2,1)}, bf16[512,1536]{1,0:T(8,128)(2,1)}, u32[]{:S(2)}, u32[]{:S(2)}) collective-permute-start(bf16[512,1536]{1,0:T(8,128)(2,1)} %collective-permute-done.2.rest_6_), channel_id=1, source_target_pairs={{16,20},{20,16},{24,28},{28,24},{17,21},{21,17},{25,29},{29,25},{1... | collective-permute-start | bytes 4718600 | tf_op jit(solution)/shard_map/ppermute | solution.py:239
  241.7 19.6 %copy-start.15 = (bf16[512,1536]{1,0:T(8,128)(2,1)}, bf16[512,1536]{1,0:T(8,128)(2,1)S(1)}, u32[]{:S(2)}) copy-start(bf16[512,1536]{1,0:T(8,128)(2,1)S(1)} %collective-permute-done.13.rest_5_) | copy-start | bytes 4718596
  241.7 83.2 %collective-permute-start.15 = (bf16[512,1536]{1,0:T(8,128)(2,1)}, bf16[512,1536]{1,0:T(8,128)(2,1)}, u32[]{:S(2)}, u32[]{:S(2)}) collective-permute-start(bf16[512,1536]{1,0:T(8,128)(2,1)} %collective-permute-done.3.rest_7_), channel_id=1, source_target_pairs={{0,4},{4,0},{8,12},{12,8},{1,5},{5,1},{9,13},{13,9},{2,6},{6,2},{1... | collective-permute-start | bytes 4718600 | tf_op jit(solution)/shard_map/ppermute | solution.py:239
  244.2 55.0 %collective-permute-start.10 = (bf16[256,1536]{1,0:T(8,128)(2,1)}, bf16[256,1536]{1,0:T(8,128)(2,1)}, u32[]{:S(2)}, u32[]{:S(2)}) collective-permute-start(bf16[256,1536]{1,0:T(8,128)(2,1)} %collective-permute-done.9.rest_3_), channel_id=1, source_target_pairs={{8,0},{12,4},{16,8},{20,12},{9,1},{13,5},{17,9},{21,13},{10,2},{14... | collective-permute-start | bytes 2359304 | tf_op jit(solution)/shard_map/ppermute | solution.py:256
  259.5 71.4 %collective-permute-start.16 = (bf16[512,1536]{1,0:T(8,128)(2,1)}, bf16[512,1536]{1,0:T(8,128)(2,1)}, u32[]{:S(2)}, u32[]{:S(2)}) collective-permute-start(bf16[512,1536]{1,0:T(8,128)(2,1)} %collective-permute-done.4.rest_10_), channel_id=1, source_target_pairs={{24,28},{28,24},{25,29},{29,25},{26,30},{30,26},{27,31},{31,27}} | collective-permute-start | bytes 4718600 | tf_op jit(solution)/shard_map/ppermute | solution.py:239
  262.2 69.4 %collective-permute-start.17 = (bf16[512,1536]{1,0:T(8,128)(2,1)}, bf16[512,1536]{1,0:T(8,128)(2,1)}, u32[]{:S(2)}, u32[]{:S(2)}) collective-permute-start(bf16[512,1536]{1,0:T(8,128)(2,1)} %collective-permute-done.5.rest_11_), channel_id=1, source_target_pairs={{0,4},{4,0},{1,5},{5,1},{2,6},{6,2},{3,7},{7,3}} | collective-permute-start | bytes 4718600 | tf_op jit(solution)/shard_map/ppermute | solution.py:239
  299.2 22.6 %collective-permute-start.6 = (bf16[16,2048]{1,0:T(8,128)(2,1)S(1)}, bf16[16,2048]{1,0:T(8,128)(2,1)S(1)}, u32[]{:S(2)}, u32[]{:S(2)}) collective-permute-start(bf16[16,2048]{1,0:T(8,128)(2,1)S(1)} %slice.4), channel_id=1, source_target_pairs={{0,4},{4,8},{8,12},{12,16},{16,20},{20,24},{24,28},{1,5},{5,9},{9,... | collective-permute-start | bytes 196616 | tf_op jit(solution)/shard_map/ppermute | solution.py:24
  321.8 4.5 %collective-permute-start.19 = (bf16[256,1536]{1,0:T(8,128)(2,1)}, bf16[256,1536]{1,0:T(8,128)(2,1)}, u32[]{:S(2)}, u32[]{:S(2)}) collective-permute-start(bf16[256,1536]{1,0:T(8,128)(2,1)} %copy-done.1), channel_id=1, source_target_pairs={{8,12},{12,8},{16,20},{20,16},{24,28},{28,24},{9,13},{13,9},{17,21... | collective-permute-start | bytes 2359304 | tf_op jit(solution)/shard_map/ppermute | solution.py:239
  323.4 10.2 %collective-permute-start.23 = (bf16[256,1536]{1,0:T(8,128)(2,1)}, bf16[256,1536]{1,0:T(8,128)(2,1)}, u32[]{:S(2)}, u32[]{:S(2)}) collective-permute-start(bf16[256,1536]{1,0:T(8,128)(2,1)} %copy-done.16), channel_id=1, source_target_pairs={{16,24},{20,28},{17,25},{21,29},{18,26},{22,30},{19,27},{23,31}} | collective-permute-start | bytes 2359304 | tf_op jit(solution)/shard_map/ppermute | solution.py:255
  324.9 27.3 %collective-permute-start.24 = (bf16[256,1536]{1,0:T(8,128)(2,1)}, bf16[256,1536]{1,0:T(8,128)(2,1)}, u32[]{:S(2)}, u32[]{:S(2)}) collective-permute-start(bf16[256,1536]{1,0:T(8,128)(2,1)} %collective-permute-done.10.rest_7_), channel_id=1, source_target_pairs={{8,0},{12,4},{9,1},{13,5},{10,2},{14,6},{11,3},{15,7}} | collective-permute-start | bytes 2359304 | tf_op jit(solution)/shard_map/ppermute | solution.py:256
  326.3 56.9 %copy-start = (bf16[256,1536]{1,0:T(8,128)(2,1)S(1)}, bf16[256,1536]{1,0:T(8,128)(2,1)}, u32[]{:S(2)}) copy-start(bf16[256,1536]{1,0:T(8,128)(2,1)} %rest_0_) | copy-start | bytes 2359300
  326.3 56.9 %copy-start.2 = (bf16[256,1536]{1,0:T(8,128)(2,1)S(1)}, bf16[256,1536]{1,0:T(8,128)(2,1)}, u32[]{:S(2)}) copy-start(bf16[256,1536]{1,0:T(8,128)(2,1)} %copy-done.1) | copy-start | bytes 2359300
  326.3 56.9 %copy-start.4 = (bf16[256,1536]{1,0:T(8,128)(2,1)S(1)}, bf16[256,1536]{1,0:T(8,128)(2,1)}, u32[]{:S(2)}) copy-start(bf16[256,1536]{1,0:T(8,128)(2,1)} %copy-done.3) | copy-start | bytes 2359300
  326.3 54.3 %collective-permute-start.20 = (bf16[256,1536]{1,0:T(8,128)(2,1)}, bf16[256,1536]{1,0:T(8,128)(2,1)S(1)}, u32[]{:S(2)}, u32[]{:S(2)}) collective-permute-start(bf16[256,1536]{1,0:T(8,128)(2,1)} %collective-permute-done.9.rest_3_), channel_id=1, source_target_pairs={{0,4},{4,0},{8,12},{12,8},{16,20},{20,16},{1,5},{5,1},{9,13},{13,9... | collective-permute-start | bytes 2359304 | tf_op jit(solution)/shard_map/ppermute | solution.py:239
  330.9 49.7 %collective-permute-start.21 = (bf16[256,1536]{1,0:T(8,128)(2,1)}, bf16[256,1536]{1,0:T(8,128)(2,1)S(1)}, u32[]{:S(2)}, u32[]{:S(2)}) collective-permute-start(bf16[256,1536]{1,0:T(8,128)(2,1)} %copy-done.16), channel_id=1, source_target_pairs={{16,20},{20,16},{24,28},{28,24},{17,21},{21,17},{25,29},{29,25},{1... | collective-permute-start | bytes 2359304 | tf_op jit(solution)/shard_map/ppermute | solution.py:239
  331.6 49.0 %collective-permute-start.22 = (bf16[256,1536]{1,0:T(8,128)(2,1)}, bf16[256,1536]{1,0:T(8,128)(2,1)S(1)}, u32[]{:S(2)}, u32[]{:S(2)}) collective-permute-start(bf16[256,1536]{1,0:T(8,128)(2,1)} %collective-permute-done.10.rest_7_), channel_id=1, source_target_pairs={{0,4},{4,0},{8,12},{12,8},{1,5},{5,1},{9,13},{13,9},{2,6},{6,2},{1... | collective-permute-start | bytes 2359304 | tf_op jit(solution)/shard_map/ppermute | solution.py:239
  333.5 47.1 %collective-permute-start.25 = (bf16[256,1536]{1,0:T(8,128)(2,1)}, bf16[256,1536]{1,0:T(8,128)(2,1)S(1)}, u32[]{:S(2)}, u32[]{:S(2)}) collective-permute-start(bf16[256,1536]{1,0:T(8,128)(2,1)} %collective-permute-done.23.rest_10_), channel_id=1, source_target_pairs={{24,28},{28,24},{25,29},{29,25},{26,30},{30,26},{27,31},{31,27}} | collective-permute-start | bytes 2359304 | tf_op jit(solution)/shard_map/ppermute | solution.py:239
  352.2 28.5 %collective-permute-start.26 = (bf16[256,1536]{1,0:T(8,128)(2,1)}, bf16[256,1536]{1,0:T(8,128)(2,1)S(1)}, u32[]{:S(2)}, u32[]{:S(2)}) collective-permute-start(bf16[256,1536]{1,0:T(8,128)(2,1)} %collective-permute-done.24.rest_11_), channel_id=1, source_target_pairs={{0,4},{4,0},{1,5},{5,1},{2,6},{6,2},{3,7},{7,3}} | collective-permute-start | bytes 2359304 | tf_op jit(solution)/shard_map/ppermute | solution.py:239
  380.6 1.1 copy-start.18
  380.6 1.3 copy-start.19
  380.7 1.6 copy-start.20
  382.3 0.9 copy-start.21
  398.7 4.5 %collective-permute-start.27 = (bf16[2,256,2048]{2,1,0:T(8,128)(2,1)}, bf16[2,256,2048]{2,1,0:T(8,128)(2,1)}, u32[]{:S(2)}, u32[]{:S(2)}) collective-permute-start(bf16[2,256,2048]{2,1,0:T(8,128)(2,1)} %dynamic-slice_bitcast_fusion), channel_id=1, source_target_pairs={{0,1},{1,0},{2,3},{3,2},{4,5},{5,4},{6,7},{7,6},{8,9},{9,8},{10,11... | collective-permute-start | bytes 6291464 | tf_op jit(solution)/shard_map/ppermute | solution.py:612
  405.2 25.3 %collective-permute-start.28 = (bf16[256,2048]{1,0:T(8,128)(2,1)S(1)}, bf16[256,2048]{1,0:T(8,128)(2,1)S(1)}, u32[]{:S(2)}, u32[]{:S(2)}) collective-permute-start(bf16[256,2048]{1,0:T(8,128)(2,1)S(1)} %fusion), channel_id=1, source_target_pairs={{0,2},{1,3},{2,0},{3,1},{4,6},{5,7},{6,4},{7,5},{8,10},{9,11},{10,... | collective-permute-start | bytes 3145736 | tf_op jit(solution)/shard_map/ppermute | solution.py:620
  (4 other events, 3.6 us)
Sparse Core Ops, SparseCore 0:
  170.8 40.0 all-gather.1
